TPU v7x, 32 devices: a whole 2x2x4 slice. The times are simulated.
32 devices in a mesh: ep: 4 (over y, x), tp: 8 (over z, core).
Axes of the slice: x: 2, y: 2, z: 4, core: 2. Of those that a mesh axis runs over, the one named last changes fastest.
Arguments:
- queries: bfloat16 [4096, 2048], P('ep', 'tp'), may hold values from -200 to 200
- key_rows: bfloat16 [4096, 1024], P('ep', 'tp'), may hold values from -6 to 6
- value_rows: bfloat16 [4096, 1024], P('ep', 'tp'), may hold values from -24 to 24
- sink_logits: float32 [32], P('tp'), may hold values from 2 to 6
- out_weight: bfloat16 [2048, 2048], P('tp'), may hold values from -0.125 to 0.125
- expert_input: bfloat16 [3072, 2048], P(('ep', 'tp')), may hold values from -6 to 6
- norm_gain: float32 [2048], replicated, may hold values from 0.1 to 1.9
- group_ids: int32 [3072, 1], P(('ep', 'tp')), may hold values from 0 to 3; in each aligned block of 96 rows (0 to 95, 96 to 191, ...) at most 30 rows name the same one
- route_weight: float32 [3072, 2], P(('ep', 'tp')), may hold values from 0.2 to 1
- gate_weight: bfloat16 [8, 2048, 4096], P('ep', None, 'tp'), may hold values from -0.125 to 0.125
- up_weight: bfloat16 [8, 2048, 4096], P('ep', None, 'tp'), may hold values from -0.125 to 0.125
- down_weight: bfloat16 [8, 4096, 2048], P('ep', 'tp'), may hold values from -0.09375 to 0.09375
Outputs:
- attn_output: bfloat16 [4096, 2048], P(('ep', 'tp'))
- expert_output: bfloat16 [3072, 2048], P(('ep', 'tp'))
Inputs may be any that keep to these rules, and one draw needn't show every extreme that they name: `group_ids`: in the rows of one device (aligned blocks of 96 rows), no group is named by more than 30 rows, and in every draw some group is named by exactly 30 rows of some block.
All inputs are finite; a program needn't handle non-finite values.
Results may differ from a plain program's by a relative error of at most 0.02.
Values may be sent and summed in bfloat16 or wider, within the bound.
No kernel may reach another device: no remote copies, remote signals or barrier semaphores. Data moves between devices by JAX's collectives and lax.ppermute only.
A program may use at most 128 MiB of HBM per device.

v0:
```python
import math

import jax
import jax.numpy as jnp
from jax import lax
from jax.sharding import PartitionSpec as P

D = 2048
HD = 64
WINDOW = 128
EXP_DEV = 2


theta_base = 10000.0
norm_eps = 1e-06
neg_large = -1e30


def shifted(shard, axis, by):
    length = lax.axis_size(axis)
    pairs = [(i, i + by) for i in range(length) if 0 <= i + by < length]
    return lax.ppermute(shard, axis, pairs)


def rotate(tensor, positions):
    halfway = tensor.shape[-1] // 2
    frequency = theta_base ** (-(jnp.arange(halfway, dtype=jnp.float32) * 2.0) / tensor.shape[-1])
    angles = positions.astype(jnp.float32)[:, None] * frequency[None, :]
    cosine = jnp.cos(angles)[:, None, :]
    sine_part = jnp.sin(angles)[:, None, :]
    front_part = tensor[..., :halfway]
    back_part = tensor[..., halfway:]
    return jnp.concatenate(
        [front_part * cosine - back_part * sine_part, back_part * cosine + front_part * sine_part],
        axis=-1,
    )


def banded(earlier, current, nblocks):
    kv_here = current.shape[1]
    joined = jnp.concatenate([earlier, current[: current.shape[0] - WINDOW]], axis=0)
    joined = joined.reshape(nblocks, WINDOW, kv_here, HD)
    return jnp.concatenate([joined, current.reshape(nblocks, WINDOW, kv_here, HD)], axis=1)


def attention(queries, key_rows, value_rows, sink_logits, out_weight):
    seg_rows = queries.shape[0]
    heads_here = sink_logits.shape[0]
    kv_here = key_rows.shape[1] // HD
    per_group = heads_here // kv_here
    nblocks = seg_rows // WINDOW
    offset = lax.axis_index("ep") * seg_rows
    positions = offset + jnp.arange(seg_rows, dtype=jnp.int32)
    rot_query = rotate(
        queries.astype(jnp.float32).reshape(seg_rows, heads_here, HD), positions
    ).astype(jnp.bfloat16)
    rot_key = rotate(key_rows.astype(jnp.float32).reshape(seg_rows, kv_here, HD), positions).astype(
        jnp.bfloat16
    )
    value_heads = value_rows.reshape(seg_rows, kv_here, HD)
    tails = jnp.stack([rot_key[seg_rows - WINDOW :], value_heads[seg_rows - WINDOW :]]).reshape(
        2, WINDOW, kv_here * HD
    )
    before = shifted(tails, "ep", 1).reshape(2, WINDOW, kv_here, HD)
    key_band = banded(before[0], rot_key, nblocks)
    value_band = banded(before[1], value_heads, nblocks)
    grouped_query = rot_query.reshape(nblocks, WINDOW, kv_here, per_group, HD)
    score_scale = 1.0 / math.sqrt(HD)
    scores = (
        jnp.einsum("nqkgd,nskd->nkgqs", grouped_query, key_band, preferred_element_type=jnp.float32)
        * score_scale
    )
    row_ids = jnp.arange(WINDOW, dtype=jnp.int32)[:, None]
    col_ids = jnp.arange(2 * WINDOW, dtype=jnp.int32)[None, :]
    lagged = row_ids + WINDOW - col_ids
    key_pos = (
        offset
        + (jnp.arange(nblocks, dtype=jnp.int32) * WINDOW)[:, None, None]
        - WINDOW
        + col_ids[None]
    )
    allowed = (lagged >= 0)[None] & (lagged < WINDOW)[None] & (key_pos >= 0)
    scores = jnp.where(allowed[:, None, None], scores, neg_large)
    sink_col = sink_logits.reshape(1, kv_here, per_group, 1, 1)
    top_val = jnp.maximum(jnp.max(scores, axis=-1, keepdims=True), sink_col)
    expo = jnp.exp(scores - top_val)
    denom = jnp.sum(expo, axis=-1, keepdims=True) + jnp.exp(sink_col - top_val)
    probs = (expo / denom).astype(jnp.bfloat16)
    attended = jnp.einsum(
        "nkgqs,nskd->nqkgd", probs, value_band, preferred_element_type=jnp.float32
    )
    attended = attended.astype(jnp.bfloat16).reshape(seg_rows, heads_here * HD)
    return lax.psum_scatter(
        jnp.dot(attended, out_weight, preferred_element_type=jnp.float32).astype(jnp.bfloat16),
        "tp",
        scatter_dimension=0,
        tiled=True,
    )


def experts(expert_input, norm_gain, group_ids, route_weight, gate_weight, up_weight, down_weight):
    token_count = expert_input.shape[0]
    n_groups = lax.axis_size("ep")
    capacity = max(2, token_count * 5 // (4 * n_groups))
    local_slots = n_groups * capacity
    as_float = expert_input.astype(jnp.float32)
    normed = (
        as_float
        * lax.rsqrt(jnp.mean(as_float * as_float, axis=-1, keepdims=True) + norm_eps)
        * norm_gain
    ).astype(jnp.bfloat16)
    chosen = group_ids[:, 0]
    onehot = (chosen[:, None] == jnp.arange(n_groups, dtype=jnp.int32)[None, :]).astype(jnp.int32)
    ranks = jnp.sum((jnp.cumsum(onehot, axis=0) - onehot) * onehot, axis=1)
    slot_of = chosen * capacity + ranks
    picker = (jnp.arange(local_slots, dtype=jnp.int32)[:, None] == slot_of[None, :]).astype(
        jnp.bfloat16
    )
    send_rows = jnp.dot(picker, normed, preferred_element_type=jnp.float32).astype(jnp.bfloat16)
    send_shares = jnp.dot(
        picker, route_weight.astype(jnp.bfloat16), preferred_element_type=jnp.float32
    ).astype(jnp.bfloat16)
    got_rows, got_shares = (
        lax.all_to_all(
            send_rows.reshape(n_groups, capacity, D), "ep", split_axis=0, concat_axis=0, tiled=True
        ),
        lax.all_to_all(
            send_shares.reshape(n_groups, capacity, EXP_DEV),
            "ep",
            split_axis=0,
            concat_axis=0,
            tiled=True,
        ),
    )
    all_rows, all_shares = (
        lax.all_gather(got_rows.reshape(local_slots, D), "tp", axis=0, tiled=True),
        lax.all_gather(got_shares.reshape(local_slots, EXP_DEV), "tp", axis=0, tiled=True),
    )
    gate_val = jnp.einsum("rd,edf->ref", all_rows, gate_weight, preferred_element_type=jnp.float32)
    up_val = jnp.einsum("rd,edf->ref", all_rows, up_weight, preferred_element_type=jnp.float32)
    hidden = (jax.nn.silu(gate_val) * up_val * all_shares.astype(jnp.float32)[:, :, None]).astype(
        jnp.bfloat16
    )
    combined = lax.psum_scatter(
        jnp.einsum("ref,efd->rd", hidden, down_weight, preferred_element_type=jnp.float32).astype(
            jnp.bfloat16
        ),
        "tp",
        scatter_dimension=0,
        tiled=True,
    )
    back_rows = lax.all_to_all(
        combined.reshape(n_groups, capacity, D), "ep", split_axis=0, concat_axis=0, tiled=True
    )
    gathered = jnp.einsum(
        "sr,sd->rd", picker, back_rows.reshape(local_slots, D), preferred_element_type=jnp.float32
    )
    return gathered.astype(jnp.bfloat16)


def body(
    queries,
    key_rows,
    value_rows,
    sink_logits,
    out_weight,
    expert_input,
    norm_gain,
    group_ids,
    route_weight,
    gate_weight,
    up_weight,
    down_weight,
):
    attn_output = attention(queries, key_rows, value_rows, sink_logits, out_weight)
    expert_output = experts(
        expert_input, norm_gain, group_ids, route_weight, gate_weight, up_weight, down_weight
    )
    return (attn_output, expert_output)


def solution(mesh):
    placed = (
        P("ep", "tp"),
        P("ep", "tp"),
        P("ep", "tp"),
        P("tp"),
        P("tp", None),
        P(("ep", "tp"), None),
        P(),
        P(("ep", "tp"), None),
        P(("ep", "tp"), None),
        P("ep", None, "tp"),
        P("ep", None, "tp"),
        P("ep", "tp", None),
    )
    return jax.shard_map(
        body,
        mesh=mesh,
        in_specs=placed,
        out_specs=(P(("ep", "tp"), None), P(("ep", "tp"), None)),
        check_vma=False,
    )
```

profile of v0, /device:TPU:0, one launch (start us, length us, event | category | flops | bytes accessed | tf_op | source)
XLA Modules:
  0.0 199.8 jit_solution(12922667364320955399)
XLA Ops:
  7.2 1.2 fusion.13
  8.5 0.7 fusion.36
  9.4 0.8 select_reduce_fusion
  10.2 0.7 multiply_add_fusion
  10.9 1.4 convolution_convert_fusion.1
  12.4 13.5 %all_to_all.15 = bf16[4,30,2048]{2,1,0:T(8,128)(2,1)S(1)} all-to-all(bf16[4,30,2048]{2,1,0:T(8,128)(2,1)S(1)} %reshape.230), channel_id=1, replica_groups=mesh['ep'=4,'tp'=8] {'ep'}, dimensions={0} | all-to-all | bytes 983040 | tf_op jit(solution)/shard_map/all_to_all | solution.py:124
  25.9 0.9 reshape.231
  27.2 7.0 %all_to_all.16 = bf16[4,30,2]{1,2,0:T(2,128)(2,1)S(1)} all-to-all(bf16[4,30,2]{1,2,0:T(2,128)(2,1)S(1)} %copy.77), channel_id=1, replica_groups=mesh['ep'=4,'tp'=8] {'ep'}, dimensions={0} | all-to-all | bytes 960 | tf_op jit(solution)/shard_map/all_to_all | solution.py:127
  34.3 12.4 %all-gather = bf16[8,120,2]{1,2,0:T(2,128)(2,1)S(1)} all-gather(bf16[1,120,2]{1,2,0:T(2,128)(2,1)S(1)} %reshape.240), channel_id=1, replica_groups=mesh['ep'=4,'tp'=8] {'tp'}, dimensions={0}, use_global_device_ids=true | all-gather | bytes 4320 | tf_op jit(solution)/shard_map/all_gather | solution.py:137
  46.7 24.8 %all-gather.3.cloned.1.call-done = bf16[960,2048]{1,0:T(8,128)(2,1)} async-done(((bf16[120,2048]{1,0:T(8,128)(2,1)}), bf16[960,2048]{1,0:T(8,128)(2,1)}) %all-gather.3.cloned.1.call-update) | async-done | bytes 3932176 | tf_op jit(solution)/shard_map/all_gather | solution.py:136
  71.5 9.6 %fusion = f32[960,2,512]{2,0,1:T(8,128)} fusion(bf16[2,2048,512]{2,1,0:T(8,128)(2,1)} %param.22, bf16[960,2048]{1,0:T(8,128)(2,1)} %all-gather.3.cloned.1.call-done), kind=kOutput, calls=%fused_computation.4 | convolution fusion | flops 4026531840 | bytes 12058624 | tf_op jit(solution)/shard_map/rd,edf->ref/dot_general | solution.py:140
  81.0 14.8 %bitcast_convert_fusion = bf16[960,2048]{1,0:T(8,128)(2,1)} fusion(bf16[2,512,2048]{2,1,0:T(8,128)(2,1)} %param.23, f32[960,2,512]{2,0,1:T(8,128)} %fusion, bf16[2,2048,512]{2,1,0:T(8,128)(2,1)} %param.21, bf16[960,2048]{1,0:T(8,128)(2,1)} %all-gather.3.cloned.1.call-done, f32[960,2]{0,1:T(2,128)S(1)} %reshape.242), kind=kOutput, calls=%fused_computation | convolution fusion | flops 8061911040 | bytes 20192768 | tf_op jit(solution)/shard_map/ref,efd->rd/dot_general | solution.py:145
  96.1 0.7 copy-done.3
  97.1 0.5 multiply_cosine_fusion
  97.7 0.6 pad_maximum_fusion.1
  98.3 3.5 %collective-permute-start = (bf16[2,128,128]{1,2,0:T(8,128)(2,1)}, bf16[2,128,128]{1,2,0:T(8,128)(2,1)S(1)}, u32[]{:S(2)}, u32[]{:S(2)}) collective-permute-start(bf16[2,128,128]{1,2,0:T(8,128)(2,1)} %pad_maximum_fusion.1), channel_id=1, source_target_pairs={{0,8},{8,16},{16,24},{1,9},{9,17},{17,25},{2,10},{10,18},{18,26},{... | collective-permute-start | bytes 196616 | tf_op jit(solution)/shard_map/ppermute | solution.py:22
  101.9 0.2 copy.72
  102.4 0.7 copy_bitcast_fusion.2
  103.2 0.3 broadcast_and_fusion
  103.6 0.2 reshape.248
  103.9 0.2 copy.86
  104.3 0.4 copy.68
  104.8 1.8 fusion.5
  106.7 1.0 fusion.4
  107.8 1.2 fusion.10
  109.0 0.3 copy.76
  109.4 3.2 %convolution_convert_fusion = bf16[1024,2048]{1,0:T(8,128)(2,1)} fusion(bf16[256,2048]{1,0:T(8,128)(2,1)S(1)} %copy-done, bf16[32,8,8,128]{3,2,1,0:T(8,128)(2,1)S(1)} %bitcast.99), kind=kOutput, calls=%fused_computation.9 | convolution fusion | flops 1075838976 | bytes 5767168 | tf_op jit(solution)/shard_map/dot_general | solution.py:94
  112.6 29.7 %reduce-scatter.5.cloned.1.call-done = bf16[120,2048]{1,0:T(8,128)(2,1)} async-done(((bf16[960,2048]{1,0:T(8,128)(2,1)}), bf16[120,2048]{1,0:T(8,128)(2,1)}) %reduce-scatter.5.cloned.1.call-update) | async-done | bytes 491536 | tf_op jit(solution)/shard_map/reduce_scatter | solution.py:144
  142.3 1.2 reshape.234
  143.5 10.6 %all_to_all.17 = bf16[4,30,2048]{2,1,0:T(8,128)(2,1)S(1)} all-to-all(bf16[4,30,2048]{2,1,0:T(8,128)(2,1)S(1)} %reshape.234), channel_id=1, replica_groups=mesh['ep'=4,'tp'=8] {'ep'}, dimensions={0} | all-to-all | bytes 983040 | tf_op jit(solution)/shard_map/all_to_all | solution.py:152
  154.2 1.1 convolution_convert_fusion.2
  155.2 38.0 %reduce-scatter.3.cloned.1.call-done = bf16[128,2048]{1,0:T(8,128)(2,1)} async-done(((bf16[1024,2048]{1,0:T(8,128)(2,1)}), bf16[128,2048]{1,0:T(8,128)(2,1)}) %reduce-scatter.3.cloned.1.call-update) | async-done | bytes 524304 | tf_op jit(solution)/shard_map/reduce_scatter | solution.py:93
  (56 shorter events, 2.4 us)
Async XLA Ops:
  7.2 102.2 %copy-start = (bf16[256,2048]{1,0:T(8,128)(2,1)S(1)}, bf16[256,2048]{1,0:T(8,128)(2,1)}, u32[]{:S(2)}) copy-start(bf16[256,2048]{1,0:T(8,128)(2,1)} %param.16) | copy-start | bytes 3145732
  7.2 19.7 %copy-start.4 = (f32[96,2]{0,1:T(2,128)S(1)}, f32[96,2]{0,1:T(2,128)}, u32[]{:S(2)}) copy-start(f32[96,2]{0,1:T(2,128)} %param.20) | copy-start | bytes 2308
  7.2 64.3 %all-gather.3.cloned.1.call-start = ((), (), s32[]{:S(2)}) async-start(), calls=%async_computation.6 | async-start | bytes 4423680 | tf_op jit(solution)/shard_map/all_gather | solution.py:136
  26.9 115.4 %reduce-scatter.5.cloned.1.call-start = ((), (), s32[]{:S(2)}) async-start(), calls=%async_computation.7 | async-start | bytes 4423680 | tf_op jit(solution)/shard_map/reduce_scatter | solution.py:144
  81.0 14.9 %slice-start = ((bf16[1024,128]{1,0:T(8,128)(2,1)}), bf16[128,128]{1,0:T(8,128)(2,1)S(1)}, s32[]{:S(2)}) async-start(bf16[1024,128]{1,0:T(8,128)(2,1)} %param.14), calls=%async_computation.8 | async-start | bytes 65536 | tf_op jit(solution)/shard_map/slice | solution.py:61
  95.9 0.9 copy-start.3
  95.9 6.0 %copy-start.2 = (bf16[1024,256]{1,0:T(8,128)(2,1)S(1)}, bf16[1024,256]{1,0:T(8,128)(2,1)}, u32[]{:S(2)}) copy-start(bf16[1024,256]{1,0:T(8,128)(2,1)} %param.12) | copy-start | bytes 1572868
  95.9 97.4 %reduce-scatter.3.cloned.1.call-start = ((), (), s32[]{:S(2)}) async-start(), calls=%async_computation.5 | async-start | bytes 4718592 | tf_op jit(solution)/shard_map/reduce_scatter | solution.py:93
  97.0 6.6 %copy-start.1 = (bf16[1024,128]{1,0:T(8,128)(2,1)S(1)}, bf16[1024,128]{1,0:T(8,128)(2,1)}, u32[]{:S(2)}) copy-start(bf16[1024,128]{1,0:T(8,128)(2,1)} %param.14) | copy-start | bytes 786436
  97.0 6.8 %copy-start.5 = (f32[4]{0:T(128)S(1)}, f32[4]{0:T(128)}, u32[]{:S(2)}) copy-start(f32[4]{0:T(128)} %param.15) | copy-start | bytes 52
  97.0 6.9 %slice-start.1 = ((bf16[1024,128]{1,0:T(8,128)(2,1)}), bf16[896,128]{1,0:T(8,128)(2,1)S(1)}, s32[]{:S(2)}) async-start(bf16[1024,128]{1,0:T(8,128)(2,1)} %param.14), calls=%async_computation.9 | async-start | bytes 458752 | tf_op jit(solution)/shard_map/slice | solution.py:41
  98.3 6.3 %collective-permute-start = (bf16[2,128,128]{1,2,0:T(8,128)(2,1)}, bf16[2,128,128]{1,2,0:T(8,128)(2,1)S(1)}, u32[]{:S(2)}, u32[]{:S(2)}) collective-permute-start(bf16[2,128,128]{1,2,0:T(8,128)(2,1)} %pad_maximum_fusion.1), channel_id=1, source_target_pairs={{0,8},{8,16},{16,24},{1,9},{9,17},{17,25},{2,10},{10,18},{18,26},{... | collective-permute-start | bytes 196616 | tf_op jit(solution)/shard_map/ppermute | solution.py:22
Sparse Core Ops, SparseCore 0:
  27.0 44.4 all-gather.2
  96.0 46.2 reduce-scatter.4
  145.2 48.0 reduce-scatter.2
where the time goes:
time: 200 us
  waiting for transfers between devices  92.5 us (46%)
  blocking collectives  43.5 us (22%)
  matrix products  33.1 us (17%)
  between operations  14.1 us (7%)
  other arithmetic  6.96 us (3%)
  local copies, waits for them, and re-layouts  5.98 us (3%)
  starting transfers between devices  3.66 us (2%)
    reduce_scatter x1, waiting for transfers between devices, attention(): lax.psum_scatter(jnp.dot(attended, out_weight, preferred_element_type=jnp...  38 us
    reduce_scatter x1, waiting for transfers between devices, experts(): lax.psum_scatter(jnp.einsum('ref,efd->rd', hidden, down_weight, preferred...  29.7 us
    all_gather x1, waiting for transfers between devices, experts(): lax.all_gather(got_rows.reshape(local_slots, D), 'tp', axis=0, tiled=True)  24.8 us
    dot_general x1, matrix products, experts(): jnp.einsum('ref,efd->rd', hidden, down_weight, preferred_element_type=jnp...  14.8 us
    all_to_all x1, blocking collectives, experts(): lax.all_to_all(send_rows.reshape(n_groups, capacity, D), 'ep', split_axis...  13.5 us
    all_gather x1, blocking collectives, experts(): lax.all_gather(got_shares.reshape(local_slots, EXP_DEV), 'tp', axis=0, ti...  12.4 us
    all_to_all x1, blocking collectives, experts(): lax.all_to_all(combined.reshape(n_groups, capacity, D), 'ep', split_axis=...  10.6 us
    dot_general x1, matrix products, experts(): jnp.einsum('rd,edf->ref', all_rows, up_weight, preferred_element_type=jnp...  9.57 us
  transfers between devices with their start and end apart: 4, of which 3 were waited for; matrix products, arithmetic and copies ran while one was open for 7% of the time, Pallas kernels for 0%

commit v1 on v0

v1 whole, which is shorter than its diff:
```python
import functools
import math

import jax
import jax.numpy as jnp
import numpy as np
from jax import lax
from jax.experimental import pallas as pl
from jax.experimental.pallas import tpu as pltpu
from jax.sharding import PartitionSpec as P


HD = 64
WINDOW = 128
EXP_DEV = 2
CORES = 2


theta_base = 10000.0
norm_eps = 1e-06
neg_large = -1e30
BF = jnp.bfloat16
F32 = jnp.float32


def gather_pairs(n, s, parity):
    pairs = []
    for link in range(parity, n - 1, 2):
        if link >= s - 1:
            pairs.append((link, link + 1))
        if link <= n - 1 - s:
            pairs.append((link + 1, link))
    return pairs


def scatter_pairs(n, s, parity):
    pairs = [(b, a) for a, b in gather_pairs(n, n - s, parity)]
    return [p for p in pairs if p not in first_hop(n)]


def first_hop(n):
    return [(0, 1), (n - 1, n - 2)]


def along(value, pairs):
    full = [(CORES * a + c, CORES * b + c) for a, b in pairs for c in range(CORES)]
    return lax.ppermute(value, "tp", full)


def core_swap(value):
    n = lax.axis_size("tp")
    return lax.ppermute(value, "tp", [(t, t ^ 1) for t in range(n)])


def slot_chunk(n, z, k):
    if k == 0:
        return z
    even = z % 2 == 0
    ec = jnp.where(even, n - 1 - z, z)
    o = n - k
    return jnp.where(
        k <= ec, jnp.where(even, z + k, z - k), jnp.where(even, z - o, z + o)
    )


def add_all(values):
    values = [v[0][v[1]] if isinstance(v, tuple) else v for v in values]
    if len(values) == 1:
        return values[0]
    return sum(v.astype(F32) for v in values).astype(BF)


class Sequence:
    def __init__(self):
        self.token = None

    def after(self, *values):
        arrays = [v[0] if isinstance(v, tuple) else v for v in values]
        arrays = lax.optimization_barrier((*arrays, self.token))[:-1]
        return [
            (a, v[1]) if isinstance(v, tuple) else a for a, v in zip(arrays, values)
        ]

    def did(self, value):
        self.token = value
        return value


class LineScatter:
    def __init__(self, n, seq):
        self.n = n
        self.seq = seq
        self.first = {}
        self.got = {}

    def send(self, values, pairs):
        out = add_all(self.seq.after(*values))
        if len(values) > 1:
            self.seq.did(out)
        return along(out, pairs)

    def start(self, s, slot):
        self.first[s] = self.send(slot, first_hop(self.n))

    def arrivals(self, s, parity):
        values = [self.got.get((s, parity))]
        if parity == 0:
            values.append(self.first.get(s))
        return [v for v in values if v is not None]

    def step(self, s, slots):
        for parity in (1, 0):
            pairs = scatter_pairs(self.n, s, parity)
            if pairs:
                slot = slots[self.n - s] if parity == 0 else slots[s]
                values = slot + self.arrivals(s - 1, 1 - parity)
                self.got[s, parity] = self.send(values, pairs)

    def finish(self, slot):
        last = self.n - 1
        return slot + self.arrivals(last, 0) + self.arrivals(last, 1)


def round_up(value, to):
    return -(-value // to) * to


def iota(shape, dim):
    return lax.broadcasted_iota(jnp.int32, shape, dim)


def routing(ids_ref, me_ref, block):
    ids = ids_ref[...].astype(F32)
    tokens = ids.shape[1]
    sq_row, sq_col = iota((tokens, tokens), 0), iota((tokens, tokens), 1)
    ids_col = jnp.sum(jnp.where(sq_row == sq_col, ids, 0.0), axis=1, keepdims=True)
    earlier = (ids_col == ids) & (sq_row < sq_col)
    rank = jnp.sum(earlier.astype(F32), axis=0, keepdims=True)
    group = (ids_ref[...] ^ me_ref[0]).astype(F32)
    slot = group * block + rank
    slot_col = jnp.sum(jnp.where(sq_row == sq_col, slot, 0.0), axis=1, keepdims=True)
    return group, rank, slot, slot_col


def dispatch_kernel(
    capacity, block, me_ref, x_ref, gain_ref, ids_ref, share_ref, k_ref, v_ref, *out_refs
):
    *out_refs, tail_ref = out_refs
    tail_ref[:WINDOW] = k_ref[...]
    tail_ref[WINDOW:] = v_ref[...]
    rows = len(out_refs) * block
    tokens = x_ref.shape[0]
    lanes = 128
    x = x_ref[...].astype(F32)
    scale = lax.rsqrt(jnp.mean(x * x, axis=-1, keepdims=True) + norm_eps)
    normed = (x * scale * gain_ref[...]).astype(BF)
    group, rank, slot, _ = routing(ids_ref, me_ref, block)
    row_id = iota((rows, tokens), 0)
    picker = (row_id.astype(F32) == slot).astype(BF)
    out = jnp.dot(picker, normed, preferred_element_type=F32)
    place = row_id % block - capacity
    same = (row_id // block).astype(F32) == group
    weight = jnp.zeros((rows, tokens), F32)
    for k in range(EXP_DEV):
        share = share_ref[k : k + 1, :].astype(BF).astype(F32)
        weight = jnp.where(same & (place == k), share, weight)
    sq_row, sq_col = iota((tokens, tokens), 0), iota((tokens, tokens), 1)
    rank_col = jnp.sum(jnp.where(sq_row == sq_col, rank, 0.0), axis=1, keepdims=True)
    by_rank = (rank_col == iota((tokens, lanes), 1).astype(F32)).astype(BF)
    tail = jnp.dot(weight.astype(BF), by_rank, preferred_element_type=F32)
    for g, out_ref in enumerate(out_refs):
        part = slice(g * block, (g + 1) * block)
        out_ref[:, :lanes] = (out[part, :lanes] + tail[part]).astype(BF)
        out_ref[:, lanes:] = out[part, lanes:].astype(BF)


def in_vmem(count):
    return [pl.BlockSpec(memory_space=pltpu.VMEM)] * count


def dispatch(me, x, gain, ids, share, keys, values, n_groups, capacity, block):
    rows, narrow = keys.shape
    gain = gain.reshape(1, -1)
    last = pl.BlockSpec((WINDOW, narrow), lambda i: (rows // WINDOW - 1, 0))

    def whole(shape):
        return pl.BlockSpec(shape, lambda i: (0, 0))

    outs = [(block, x.shape[1])] * n_groups + [(2 * WINDOW, narrow)]
    return pl.pallas_call(
        functools.partial(dispatch_kernel, capacity, block),
        grid=(1,),
        in_specs=[pl.BlockSpec(memory_space=pltpu.SMEM)]
        + [whole(v.shape) for v in (x, gain, ids, share)]
        + [last, last],
        out_specs=[whole(o) for o in outs],
        out_shape=[jax.ShapeDtypeStruct(o, BF) for o in outs],
        compiler_params=pltpu.CompilerParams(vmem_limit_bytes=60 << 20),
        name="dispatch",
    )(me, x, gain, ids, share, keys, values)


def pack_kernel(*refs):
    *parts, out_ref = refs
    block = parts[0].shape[0]
    for i, part in enumerate(parts):
        out_ref[i * block : (i + 1) * block] = part[...]


def pack(parts):
    block, width = parts[0].shape
    return pl.pallas_call(
        pack_kernel,
        in_specs=in_vmem(len(parts)),
        out_specs=in_vmem(1)[0],
        out_shape=jax.ShapeDtypeStruct((len(parts) * block, width), BF),
        compiler_params=pltpu.CompilerParams(vmem_limit_bytes=16 << 20),
        name="pack",
    )(*parts)


def combine_kernel(block, me_ref, ids_ref, *refs):
    *parts, out_ref = refs
    tokens = out_ref.shape[0]
    slot_col = routing(ids_ref, me_ref, block)[3]
    rows = jnp.concatenate([p[...] for p in parts], axis=0)
    picker = (slot_col == iota((tokens, rows.shape[0]), 1).astype(F32)).astype(BF)
    out_ref[...] = jnp.dot(picker, rows, preferred_element_type=F32).astype(BF)


def combine(me, ids, parts):
    block, width = parts[0].shape
    return pl.pallas_call(
        functools.partial(combine_kernel, block),
        in_specs=[pl.BlockSpec(memory_space=pltpu.SMEM)] + in_vmem(1 + len(parts)),
        out_shape=jax.ShapeDtypeStruct((ids.shape[1], width), BF),
        compiler_params=pltpu.CompilerParams(vmem_limit_bytes=16 << 20),
        name="combine",
    )(me, ids, *parts)


def expert_kernel(capacity, block, count, *refs):
    parts, refs = refs[:count], refs[count:]
    gate_ref, up_ref, down_ref = refs[:3]
    outs = refs[3 : 3 + count]
    x_s, h_s = refs[3 + count :]
    half = parts[0].shape[0]
    units = gate_ref.shape[2]
    for i, part in enumerate(parts):
        x_s[i * half : (i + 1) * half] = part[...]
    row, col = iota((half, half), 0), iota((half, half), 1)
    mine = iota((half, 128), 0) % block == iota((half, 128), 1)
    shares = []
    for k in range(EXP_DEV):
        take = (col == row - row % block + capacity + k).astype(BF)
        columns = []
        for part in parts:
            spread = jnp.dot(take, part[:, :128], preferred_element_type=F32)
            columns.append(jnp.sum(jnp.where(mine, spread, 0.0), axis=1, keepdims=True))
        shares.append(jnp.concatenate(columns, axis=0))
    cut = math.gcd(units, 256)
    for k in range(EXP_DEV):
        for c in range(0, units, cut):
            x = x_s[...]
            gate = jnp.dot(x, gate_ref[k, :, c : c + cut], preferred_element_type=F32)
            up = jnp.dot(x, up_ref[k, :, c : c + cut], preferred_element_type=F32)
            hidden = gate / (1.0 + jnp.exp(-gate)) * up * shares[k]
            h_s[:, k * units + c : k * units + c + cut] = hidden.astype(BF)
    width = x_s.shape[1]
    piece = math.gcd(width, 512)
    for c in range(0, width, piece):
        total = jnp.dot(h_s[...], down_ref[:, c : c + piece], preferred_element_type=F32)
        for i, out in enumerate(outs):
            out[:, c : c + piece] = total[i * half : (i + 1) * half].astype(BF)


def expert_rows(parts, gate, up, down, capacity, block):
    count = len(parts)
    half, width = parts[0].shape
    units = gate.shape[2]
    return pl.pallas_call(
        functools.partial(expert_kernel, capacity, block, count),
        in_specs=in_vmem(count + 3),
        out_specs=in_vmem(count),
        out_shape=[jax.ShapeDtypeStruct((half, width), BF)] * count,
        scratch_shapes=[
            pltpu.VMEM((count * half, width), BF),
            pltpu.VMEM((count * half, EXP_DEV * units), BF),
        ],
        cost_estimate=pl.CostEstimate(
            flops=2 * count * half * width * units * EXP_DEV * 3,
            bytes_accessed=4 * count * half * width,
            transcendentals=count * half * units * EXP_DEV,
        ),
        compiler_params=pltpu.CompilerParams(vmem_limit_bytes=24 << 20),
        name="experts",
    )(*parts, gate, up, down)


def attention_kernel(
    kv_here,
    per_group,
    many,
    order_ref,
    base_ref,
    sink_ref,
    q_ref,
    k_ref,
    v_ref,
    tail_ref,
    step_ref,
    start_ref,
    turn_ref,
    w_ref,
    *rest,
):
    span = WINDOW
    turn = turn_ref[...]
    plus_ref = rest[0] if len(rest) > 1 else None
    outs = rest[1:]
    step = pl.program_id(0)
    shape = (per_group * span, 2 * span)
    row = lax.broadcasted_iota(jnp.int32, shape, 0)
    col = lax.broadcasted_iota(jnp.int32, shape, 1)
    lag = row % span + span - col
    inside = (lag >= 0) & (lag < span)
    column = lax.broadcasted_iota(jnp.int32, (per_group * span, 1), 0) // span
    sinks = []
    for c in range(kv_here):
        sink = jnp.full((per_group * span, 1), sink_ref[c * per_group], F32)
        for g in range(1, per_group):
            sink = jnp.where(column == g, sink_ref[c * per_group + g], sink)
        sinks.append(sink)

    def rotated(x, at, scale):
        width = x.shape[1]
        cos_i, sin_i = step_ref[0, :, :width], step_ref[1, :, :width]
        base = start_ref[at]
        cos_0, sin_0 = base[0:1, :width], base[1:2, :width]
        cosine = cos_0 * cos_i - sin_0 * sin_i
        sine = sin_0 * cos_i + cos_0 * sin_i
        swapped = jnp.dot(x, turn[:width, :width], preferred_element_type=F32)
        return ((x.astype(F32) * cosine + swapped * sine) * scale).astype(BF)

    for b in range(many):
        index = order_ref[step * many + b]
        first = index == 0
        place = base_ref[0] + index
        here = pl.ds(pl.multiple_of(index * span, span), span)
        back = pl.ds(pl.multiple_of(jnp.maximum(index - 1, 0) * span, span), span)
        q = rotated(q_ref[here, :], place, 1.0 / math.sqrt(HD))
        before_k = jnp.where(first, tail_ref[:span], k_ref[back, :])
        before_v = jnp.where(first, tail_ref[span:], v_ref[back, :])
        keys = jnp.concatenate(
            [
                rotated(before_k, jnp.maximum(place - 1, 0), 1.0),
                rotated(k_ref[here, :], place, 1.0),
            ],
            axis=0,
        )
        values = jnp.concatenate([before_v, v_ref[here, :]], axis=0)
        allowed = inside & (col >= jnp.where(place == 0, span, 0))
        attended = []
        for c in range(kv_here):
            heads = [c * per_group + g for g in range(per_group)]
            rows = jnp.concatenate([q[:, h * HD : (h + 1) * HD] for h in heads], axis=0)
            key = keys[:, c * HD : (c + 1) * HD]
            scores = lax.dot_general(
                rows, key, (((1,), (1,)), ((), ())), preferred_element_type=F32
            )
            scores = jnp.where(allowed, scores, neg_large)
            top = jnp.maximum(jnp.max(scores, axis=1, keepdims=True), sinks[c])
            expo = jnp.exp(scores - top)
            denom = jnp.sum(expo, axis=1, keepdims=True) + jnp.exp(sinks[c] - top)
            mixed = jnp.dot(
                expo.astype(BF), values[:, c * HD : (c + 1) * HD], preferred_element_type=F32
            )
            mixed = (mixed / denom).astype(BF)
            attended += [mixed[g * span : (g + 1) * span] for g in range(per_group)]
        attended = jnp.concatenate(attended, axis=1)
        total = jnp.dot(attended, w_ref[...], preferred_element_type=F32)
        if plus_ref is None:
            rest[0][b] = total.astype(BF)
            continue
        total = (total + plus_ref[b].astype(F32)).astype(BF)
        for i in range(b, len(outs), many):

            @pl.when(step == i // many)
            def _(i=i):
                outs[i][...] = total


def rotary_tables(width, blocks):
    half = HD // 2
    frequency = theta_base ** (-(np.arange(half, dtype=np.float64) * 2.0) / HD)
    lanes = np.tile(frequency, width // half)[None, :]
    inside = np.arange(WINDOW)[:, None] * lanes
    starts = (np.arange(blocks) * WINDOW)[:, None] * lanes
    steps = np.stack([np.cos(inside), np.sin(inside)]).astype(np.float32)
    bases = np.stack([np.cos(starts), np.sin(starts)], axis=1).astype(np.float32)
    lane = np.arange(width)
    turn = np.zeros((width, width), np.float32)
    low = lane % HD < half
    turn[np.where(low, lane + half, lane - half), lane] = np.where(low, -1.0, 1.0)
    return steps, bases, turn


def attention_partials(
    order, base, queries, keys, values, tails, sinks, weight, blocks, plus=None
):
    width = queries.shape[1]
    narrow = keys.shape[1]
    kv_here = narrow // HD
    per_group = width // narrow
    count = order.shape[0]
    steps, bases, turn = rotary_tables(width, blocks)
    many = math.gcd(count, 2)
    operands = (
        queries,
        keys,
        values,
        tails,
        jnp.asarray(steps),
        jnp.asarray(bases),
        jnp.asarray(turn, BF),
        weight,
    )

    def fixed(x):
        return pl.BlockSpec(x.shape, lambda i, o, b, s: (0,) * len(x.shape))

    out_width = weight.shape[1]
    stack = pl.BlockSpec((many, WINDOW, out_width), lambda i, o, b, s: (i, 0, 0))
    in_specs = [fixed(x) for x in operands]
    if plus is None:
        out_specs, out_shape = stack, jax.ShapeDtypeStruct((count, WINDOW, out_width), BF)
    else:
        operands += (plus,)
        in_specs += [stack]
        out_shape = [jax.ShapeDtypeStruct((WINDOW, out_width), BF)] * count
        out_specs = [fixed(o) for o in out_shape]
    return pl.pallas_call(
        functools.partial(attention_kernel, kv_here, per_group, many),
        grid_spec=pltpu.PrefetchScalarGridSpec(
            num_scalar_prefetch=3,
            grid=(count // many,),
            in_specs=in_specs,
            out_specs=out_specs,
        ),
        out_shape=out_shape,
        cost_estimate=pl.CostEstimate(
            flops=2 * count * WINDOW * width * (weight.shape[1] + 4 * WINDOW),
            bytes_accessed=2 * weight.size + 2 * count * WINDOW * (weight.shape[1] + 2 * width),
            transcendentals=count * WINDOW * 2 * WINDOW * kv_here * per_group,
        ),
        compiler_params=pltpu.CompilerParams(vmem_limit_bytes=(60 if plus is None else 28) << 20),
        name="attention",
    )(order, base, sinks, *operands)


def body(
    queries,
    key_rows,
    value_rows,
    sink_logits,
    out_weight,
    expert_input,
    norm_gain,
    group_ids,
    route_weight,
    gate_weight,
    up_weight,
    down_weight,
):
    n_groups = lax.axis_size("ep")
    n_tp = lax.axis_size("tp")
    n = n_tp // CORES
    token_count, width = expert_input.shape
    capacity = max(2, token_count * 5 // (4 * n_groups))
    block = round_up(capacity + EXP_DEV, 8)
    e = lax.axis_index("ep")
    t = lax.axis_index("tp")
    z, core = t // CORES, t % CORES
    me = e.reshape(1)
    ids = group_ids.reshape(1, token_count)
    seq = Sequence()

    def around(part, k):
        return lax.ppermute(part, "ep", [(i, i ^ k) for i in range(n_groups)])

    *send, tails = dispatch(
        me,
        expert_input,
        norm_gain,
        ids,
        route_weight.T,
        key_rows,
        value_rows,
        n_groups,
        capacity,
        block,
    )
    seq.did(send[0])
    got = [send[0]] + [around(send[k], k) for k in range(1, n_groups)]

    before = lax.ppermute(tails, "ep", [(i, i + 1) for i in range(n_groups - 1)])
    chunk = jnp.stack([slot_chunk(n, z, k) for k in range(n)]) * CORES

    def attend(order, plus=None):
        (q,) = seq.after(queries)
        return attention_partials(
            order,
            (e * n_tp).reshape(1),
            q,
            key_rows,
            value_rows,
            before,
            sink_logits,
            out_weight,
            n_groups * n_tp,
            plus,
        )

    arrived = {}

    def gather(s):
        for parity in (1, 0):
            pairs = gather_pairs(n, s, parity)
            if pairs:
                value = own
                if s > 1:
                    (value,) = seq.after(arrived[s - 1, 1 - parity])
                arrived[s, parity] = along(value, pairs)

    slots = {}

    def prepare(s):
        for k in range(1, n):
            late = n - k if gather_pairs(n, n - k, 1) else 0
            if max(k, late) == s:
                addends = [arrived[k, 0], arrived.get((n - k, 1))]
                slot = add_all([a for a in addends if a is not None])
                slots[k] = [slot, core_swap(slot)]

    back = {}

    def experts(ks):
        for k in ks:
            parts = seq.after(*slots[k])
            done = expert_rows(parts, *weights, capacity, block)
            seq.did(done[0])
            back[k] = [done[0], core_swap(done[1])]

    own = seq.did(pack(seq.after(*got)))
    gather(1)
    slots[0] = [own, core_swap(own)]
    other = seq.did(attend(chunk + 1 - core))
    swapped = core_swap(other)
    weights = seq.after(gate_weight, up_weight, down_weight.reshape(-1, width))
    attn_scatter = LineScatter(n, seq)
    for s in range(1, n):
        todo = [k for k in slots if k not in back]
        if s == n - 1:
            experts(todo)
        else:
            gather(s + 1)
        prepare(s)
        if s == 1:
            (swapped,) = seq.after(swapped)
            mine = attend(chunk + core, swapped)
            seq.did(mine[0])
            attn = [[v] for v in mine]
            for a in range(1, n):
                attn_scatter.start(a, attn[n - a])
        elif s < n - 1:
            experts(todo[:1])
            attn_scatter.step(s, attn)
            experts(todo[1:])
    experts([k for k in slots if k not in back])
    attn_scatter.step(n - 1, attn)

    scatter = LineScatter(n, seq)
    for s in range(1, n):
        scatter.start(s, back[n - s])
    for s in range(2, n):
        scatter.step(s, back)
    attn_output = seq.did(add_all(seq.after(*attn_scatter.finish(attn[0]))))
    addends = seq.after(*scatter.finish(back[0]))
    home = []
    for k in range(n_groups):
        part = add_all([v[k * block : (k + 1) * block] for v in addends])
        home.append(around(part, k) if k else part)
    expert_output = combine(me, ids, home)
    return (attn_output, expert_output)


def solution(mesh):
    placed = (
        P("ep", "tp"),
        P("ep", "tp"),
        P("ep", "tp"),
        P("tp"),
        P("tp", None),
        P(("ep", "tp"), None),
        P(),
        P(("ep", "tp"), None),
        P(("ep", "tp"), None),
        P("ep", None, "tp"),
        P("ep", None, "tp"),
        P("ep", "tp", None),
    )
    return jax.shard_map(
        body,
        mesh=mesh,
        in_specs=placed,
        out_specs=(P(("ep", "tp"), None), P(("ep", "tp"), None)),
        check_vma=False,
    )
```

time: 200 us -> 151 us (0.76)
  starting transfers between devices: 3.66 us -> 54.2 us
  blocking collectives: 43.5 us -> 0 us
  waiting for transfers between devices: 92.5 us -> 53.2 us
  matrix products: 33.1 us -> 0 us
  Pallas kernels: 0 us -> 31.1 us
  between operations: 14.1 us -> 1.3 us
  other arithmetic: 6.96 us -> 3.92 us
    reduce_scatter x2 -> x0, waiting for transfers between devices: 67.7 us -> none  [the longest x1 38 us: attention(): lax.psum_scatter(jnp.dot(attended, out_weight, preferred_element_type=jnp...]
    ppermute x1 -> x33, waiting for transfers between devices: 0.01 us -> 53.2 us  [the longest x17 45.6 us: along(): return lax.ppermute(value, 'tp', full)]
    ppermute x1 -> x33, starting transfers between devices: 3.54 us -> 54.2 us  [the longest x17 39.6 us: along(): return lax.ppermute(value, 'tp', full)]
    dot_general x8 -> x0, matrix products: 33.1 us -> none  [the longest x1 14.8 us: experts(): jnp.einsum('ref,efd->rd', hidden, down_weight, preferred_element_type=jnp...]
    pallas_call x0 -> x9, Pallas kernels: none -> 31.1 us  [the longest x4 14.1 us: expert_rows(): pl.pallas_call(functools.partial(expert_kernel, capacity, block, count),...]
    all_to_all x3 -> x0, blocking collectives: 31.1 us -> none  [the longest x1 13.5 us: experts(): lax.all_to_all(send_rows.reshape(n_groups, capacity, D), 'ep', split_axis...]
    all_gather x1 -> x0, waiting for transfers between devices: 24.8 us -> none  [experts(): lax.all_gather(got_rows.reshape(local_slots, D), 'tp', axis=0, tiled=True)]
    all_gather x1 -> x0, blocking collectives: 12.4 us -> none  [experts(): lax.all_gather(got_shares.reshape(local_slots, EXP_DEV), 'tp', axis=0, ti...]
  transfers between devices with their start and end apart: 4 -> 33, of which waited for: 3 -> 14; matrix products, arithmetic and copies ran while one was open for 7% -> 2% of each run, Pallas kernels for 0% -> 13%
where the time goes in v1:
time: 151 us
  starting transfers between devices  54.2 us (36%)
  waiting for transfers between devices  53.2 us (35%)
  Pallas kernels  31.1 us (21%)
  local copies, waits for them, and re-layouts  6.8 us (5%)
  other arithmetic  3.92 us (3%)
    ppermute x17, waiting for transfers between devices, along(): return lax.ppermute(value, 'tp', full)  45.6 us
    ppermute x17, starting transfers between devices, along(): return lax.ppermute(value, 'tp', full)  39.6 us
    pallas_call x4, Pallas kernels, expert_rows(): pl.pallas_call(functools.partial(expert_kernel, capacity, block, count),...  14.1 us
    pallas_call x2, Pallas kernels, attention_partials(): pl.pallas_call(functools.partial(attention_kernel, kv_here, per_group, ma...  13.4 us
    ppermute x6, starting transfers between devices, around(): return lax.ppermute(part, 'ep', [(i, i ^ k) for i in range(n_groups)])  8.92 us
    unnamed x32, local copies, waits for them, and re-layouts  6.8 us
    ppermute x6, waiting for transfers between devices, around(): return lax.ppermute(part, 'ep', [(i, i ^ k) for i in range(n_groups)])  6.25 us
    ppermute x1, starting transfers between devices, body(): lax.ppermute(tails, 'ep', [(i, i + 1) for i in range(n_groups - 1)])  3.86 us
  transfers between devices with their start and end apart: 33, of which 14 were waited for; matrix products, arithmetic and copies ran while one was open for 2% of the time, Pallas kernels for 13%

profile of v1, /device:TPU:0, one launch (start us, length us, event | category | flops | bytes accessed | tf_op | source)
XLA Modules:
  0.0 150.6 jit_solution(9306014586182846922)
XLA Ops:
  0.7 2.4 %dispatch.1 = (bf16[32,2048]{1,0:T(8,128)(2,1)}, bf16[32,2048]{1,0:T(8,128)(2,1)}, bf16[32,2048]{1,0:T(8,128)(2,1)}, bf16[32,2048]{1,0:T(8,128)(2,1)}, bf16[256,128]{1,0:T(8,128)(2,1)}) custom-call(s32[1]{0:T(128)} %bitcast.5.me_ref, bf16[96,2048]{1,0:T(8,128)(2,1)} %x_ref.1, f32[1,2048]{1,0:T(1,128)} %bitcast.16, s32[1,96]{1,0:T(1,128)} %bitcast.14, ...), custom_call_target="tpu_custom_call" | custom-call | tf_op jit(solution)/shard_map/dispatch/pallas_call | solution.py:190
  3.2 3.0 %collective-permute-start = (bf16[32,2048]{1,0:T(8,128)(2,1)}, bf16[32,2048]{1,0:T(8,128)(2,1)S(1)}, u32[]{:S(2)}, u32[]{:S(2)}) collective-permute-start(bf16[32,2048]{1,0:T(8,128)(2,1)} %get-tuple-element.74), channel_id=1, source_target_pairs={{0,8},{8,0},{16,24},{24,16},{1,9},{9,1},{17,25},{25,17},{2,10},{10... | collective-permute-start | bytes 393224 | tf_op jit(solution)/shard_map/ppermute | solution.py:489
  6.1 1.5 %collective-permute-start.1 = (bf16[32,2048]{1,0:T(8,128)(2,1)}, bf16[32,2048]{1,0:T(8,128)(2,1)S(1)}, u32[]{:S(2)}, u32[]{:S(2)}) collective-permute-start(bf16[32,2048]{1,0:T(8,128)(2,1)} %get-tuple-element.75), channel_id=1, source_target_pairs={{0,16},{8,24},{16,0},{24,8},{1,17},{9,25},{17,1},{25,9},{2,18},{10... | collective-permute-start | bytes 393224 | tf_op jit(solution)/shard_map/ppermute | solution.py:489
  7.7 3.9 %collective-permute-start.3 = (bf16[256,128]{1,0:T(8,128)(2,1)}, bf16[256,128]{1,0:T(8,128)(2,1)S(1)}, u32[]{:S(2)}, u32[]{:S(2)}) collective-permute-start(bf16[256,128]{1,0:T(8,128)(2,1)} %get-tuple-element.82), channel_id=1, source_target_pairs={{0,8},{8,16},{16,24},{1,9},{9,17},{17,25},{2,10},{10,18},{18,26},{... | collective-permute-start | bytes 196616 | tf_op jit(solution)/shard_map/ppermute | solution.py:506
  12.3 1.9 %collective-permute-done.1.refs_2_ = bf16[32,2048]{1,0:T(8,128)(2,1)S(1)} collective-permute-done((bf16[32,2048]{1,0:T(8,128)(2,1)}, bf16[32,2048]{1,0:T(8,128)(2,1)S(1)}, u32[]{:S(2)}, u32[]{:S(2)}) %collective-permute-start.1) | collective-permute-done | bytes 131104 | tf_op jit(solution)/shard_map/ppermute | solution.py:489
  15.7 7.9 %attention.2 = bf16[4,128,2048]{2,1,0:T(8,128)(2,1)} custom-call(s32[4]{0:T(128)} %get-tuple-element.144.order_ref, s32[1]{0:T(128)} %bitcast.4.base_ref, f32[4]{0:T(128)} %sink_ref.3, bf16[1024,256]{1,0:T(8,128)(2,1)} %q_ref.1, bf16[1024,128]{1,0:T(8,128)(2,1)} %k_ref.5, bf16[1024,128]{1,0:T(8,128)(2,1)} %v_ref.5, bf16[256,128]{1,0:T(8,128)(2,1)} %copy-done.11, ...), custom_call_target="tpu_custom_call" | custom-call | flops 671088640 | bytes 3670016 | tf_op jit(solution)/shard_map/attention/pallas_call | solution.py:442
  23.6 1.6 %collective-permute-start.9 = (bf16[128,2048]{1,0:T(8,128)(2,1)S(1)}, bf16[128,2048]{1,0:T(8,128)(2,1)S(1)}, u32[]{:S(2)}, u32[]{:S(2)}) collective-permute-start(bf16[128,2048]{1,0:T(8,128)(2,1)S(1)} %pack.1.refs_0_), channel_id=1, source_target_pairs={{0,2},{1,3},{2,0},{3,1},{4,6},{5,7},{6,4},{7,5},{8,10},{9,11},{10,... | collective-permute-start | bytes 1572872 | tf_op jit(solution)/shard_map/ppermute | solution.py:47
  26.0 12.0 %collective-permute-done.9.refs_0_ = bf16[128,2048]{1,0:T(8,128)(2,1)S(1)} collective-permute-done((bf16[128,2048]{1,0:T(8,128)(2,1)S(1)}, bf16[128,2048]{1,0:T(8,128)(2,1)S(1)}, u32[]{:S(2)}, u32[]{:S(2)}) %collective-permute-start.9) | collective-permute-done | bytes 524320 | tf_op jit(solution)/shard_map/ppermute | solution.py:47
  41.5 5.5 %attention.3 = (bf16[128,2048]{1,0:T(8,128)(2,1)S(1)}, bf16[128,2048]{1,0:T(8,128)(2,1)S(1)}, bf16[128,2048]{1,0:T(8,128)(2,1)S(1)}, bf16[128,2048]{1,0:T(8,128)(2,1)S(1)}) custom-call(s32[4]{0:T(128)S(1)} %broadcast_add_fusion.order_ref, s32[1]{0:T(128)} %bitcast.4.base_ref, f32[4]{0:T(128)S(1)} %copy-done.15, bf16[1024,256]{1,0:T(8,128)(2,1)S(1)} %copy-done.7, ...), custom_call_target="tpu_custom_call" | custom-call | flops 671088640 | bytes 3670016 | tf_op jit(solution)/shard_map/attention/pallas_call | solution.py:442
  46.9 6.3 %collective-permute-start.5 = (bf16[128,2048]{1,0:T(8,128)(2,1)S(1)}, bf16[128,2048]{1,0:T(8,128)(2,1)S(1)}, u32[]{:S(2)}, u32[]{:S(2)}) collective-permute-start(bf16[128,2048]{1,0:T(8,128)(2,1)S(1)} %get-tuple-element.111), channel_id=1, source_target_pairs={{0,2},{1,3},{6,4},{7,5},{8,10},{9,11},{14,12},{15,13},{16,18},{17,... | collective-permute-start | bytes 1572872 | tf_op jit(solution)/shard_map/ppermute | solution.py:47
  53.3 2.4 %collective-permute-done.14 = bf16[128,2048]{1,0:T(8,128)(2,1)S(1)} collective-permute-done((bf16[128,2048]{1,0:T(8,128)(2,1)S(1)}, bf16[128,2048]{1,0:T(8,128)(2,1)S(1)}, u32[]{:S(2)}, u32[]{:S(2)}) %collective-permute-start.14) | collective-permute-done | bytes 524320 | tf_op jit(solution)/shard_map/ppermute | solution.py:47
  57.2 4.6 %collective-permute-start.8 = (bf16[128,2048]{1,0:T(8,128)(2,1)S(1)}, bf16[128,2048]{1,0:T(8,128)(2,1)S(1)}, u32[]{:S(2)}, u32[]{:S(2)}) collective-permute-start(bf16[128,2048]{1,0:T(8,128)(2,1)S(1)} %get-tuple-element.98), channel_id=1, source_target_pairs={{0,2},{1,3},{6,4},{7,5},{8,10},{9,11},{14,12},{15,13},{16,18},{17,... | collective-permute-start | bytes 1572872 | tf_op jit(solution)/shard_map/ppermute | solution.py:47
  61.9 2.2 %copy-done.1 = bf16[2,2048,512]{2,1,0:T(8,128)(2,1)S(1)} copy-done((bf16[2,2048,512]{2,1,0:T(8,128)(2,1)S(1)}, bf16[2,2048,512]{2,1,0:T(8,128)(2,1)}, u32[]{:S(2)}) %copy-start.1) | copy-done | bytes 4194328
  64.1 2.2 %copy-done.3 = bf16[2,512,2048]{2,1,0:T(8,128)(2,1)S(1)} copy-done((bf16[2,512,2048]{2,1,0:T(8,128)(2,1)S(1)}, bf16[2,512,2048]{2,1,0:T(8,128)(2,1)}, u32[]{:S(2)}) %copy-start.3) | copy-done | bytes 4194328
  66.2 3.5 %experts.4 = (bf16[128,2048]{1,0:T(8,128)(2,1)S(1)}, bf16[128,2048]{1,0:T(8,128)(2,1)S(1)}) custom-call(bf16[128,2048]{1,0:T(8,128)(2,1)S(1)} %pack.1.refs_0_, bf16[128,2048]{1,0:T(8,128)(2,1)S(1)} %collective-permute-done.6.refs_1_, bf16[2,2048,512]{2,1,0:T(8,128)(2,1)S(1)} %copy-done, bf16[2,2048,512]{2,1,0:T(8,128)(2,1)S(1)} %copy-done.1, ...), custom_call_target="tpu_custom_call" | custom-call | flops 3221225472 | bytes 2097152 | tf_op jit(solution)/shard_map/experts/pallas_call | solution.py:281
  70.8 1.3 collective-permute-done.11
  72.4 3.5 %experts.5 = (bf16[128,2048]{1,0:T(8,128)(2,1)S(1)}, bf16[128,2048]{1,0:T(8,128)(2,1)S(1)}) custom-call(bf16[128,2048]{1,0:T(8,128)(2,1)S(1)} %collective-permute-done.9.refs_0_, bf16[128,2048]{1,0:T(8,128)(2,1)S(1)} %collective-permute-done.16.refs_1_, bf16[2,2048,512]{2,1,0:T(8,128)(2,1)S(1)} %copy-done, bf16[2,2048,512]{2,1,0:T(8,128)(2,1)S(1)} %copy-done.1, ...), custom_call_target="tpu_custom_call" | custom-call | flops 3221225472 | bytes 2097152 | tf_op jit(solution)/shard_map/experts/pallas_call | solution.py:281
  75.9 3.5 %experts.6 = (bf16[128,2048]{1,0:T(8,128)(2,1)S(1)}, bf16[128,2048]{1,0:T(8,128)(2,1)S(1)}) custom-call(bf16[128,2048]{1,0:T(8,128)(2,1)S(1)} %add_convert_fusion.9.refs_0_, bf16[128,2048]{1,0:T(8,128)(2,1)S(1)} %collective-permute-done.15.refs_1_, bf16[2,2048,512]{2,1,0:T(8,128)(2,1)S(1)} %copy-done, bf16[2,2048,512]{2,1,0:T(8,128)(2,1)S(1)} %copy-done.2, ...), custom_call_target="tpu_custom_call" | custom-call | flops 3221225472 | bytes 2097152 | tf_op jit(solution)/shard_map/experts/pallas_call | solution.py:281
  80.1 3.5 %experts.7 = (bf16[128,2048]{1,0:T(8,128)(2,1)S(1)}, bf16[128,2048]{1,0:T(8,128)(2,1)S(1)}) custom-call(bf16[128,2048]{1,0:T(8,128)(2,1)S(1)} %add_convert_fusion.10.refs_0_, bf16[128,2048]{1,0:T(8,128)(2,1)S(1)} %collective-permute-done.13.refs_1_, bf16[2,2048,512]{2,1,0:T(8,128)(2,1)S(1)} %copy-done, bf16[2,2048,512]{2,1,0:T(8,128)(2,1)S(1)} %copy-done.2, ...), custom_call_target="tpu_custom_call" | custom-call | flops 3221225472 | bytes 2097152 | tf_op jit(solution)/shard_map/experts/pallas_call | solution.py:281
  85.8 2.4 %collective-permute-start.23 = (bf16[128,2048]{1,0:T(8,128)(2,1)S(1)}, bf16[128,2048]{1,0:T(8,128)(2,1)S(1)}, u32[]{:S(2)}, u32[]{:S(2)}) collective-permute-start(bf16[128,2048]{1,0:T(8,128)(2,1)S(1)} %add_convert_fusion.6), channel_id=1, source_target_pairs={{0,2},{1,3},{6,4},{7,5},{8,10},{9,11},{14,12},{15,13},{16,18},{17,... | collective-permute-start | bytes 1572872 | tf_op jit(solution)/shard_map/ppermute | solution.py:47
  88.4 1.3 collective-permute-start.25
  89.9 10.6 %collective-permute-done.23 = bf16[128,2048]{1,0:T(8,128)(2,1)S(1)} collective-permute-done((bf16[128,2048]{1,0:T(8,128)(2,1)S(1)}, bf16[128,2048]{1,0:T(8,128)(2,1)S(1)}, u32[]{:S(2)}, u32[]{:S(2)}) %collective-permute-start.23) | collective-permute-done | bytes 524320 | tf_op jit(solution)/shard_map/ppermute | solution.py:47
  101.5 6.4 %collective-permute-start.18 = (bf16[128,2048]{1,0:T(8,128)(2,1)S(1)}, bf16[128,2048]{1,0:T(8,128)(2,1)S(1)}, u32[]{:S(2)}, u32[]{:S(2)}) collective-permute-start(bf16[128,2048]{1,0:T(8,128)(2,1)S(1)} %get-tuple-element.115), channel_id=1, source_target_pairs={{0,2},{1,3},{6,4},{7,5},{8,10},{9,11},{14,12},{15,13},{16,18},{17,... | collective-permute-start | bytes 1572872 | tf_op jit(solution)/shard_map/ppermute | solution.py:47
  109.3 2.5 %collective-permute-done.25 = bf16[128,2048]{1,0:T(8,128)(2,1)S(1)} collective-permute-done((bf16[128,2048]{1,0:T(8,128)(2,1)S(1)}, bf16[128,2048]{1,0:T(8,128)(2,1)S(1)}, u32[]{:S(2)}, u32[]{:S(2)}) %collective-permute-start.25) | collective-permute-done | bytes 524320 | tf_op jit(solution)/shard_map/ppermute | solution.py:47
  112.7 7.4 %collective-permute-start.28 = (bf16[128,2048]{1,0:T(8,128)(2,1)S(1)}, bf16[128,2048]{1,0:T(8,128)(2,1)S(1)}, u32[]{:S(2)}, u32[]{:S(2)}) collective-permute-start(bf16[128,2048]{1,0:T(8,128)(2,1)S(1)} %add_convert_fusion.4), channel_id=1, source_target_pairs={{0,2},{1,3},{6,4},{7,5},{8,10},{9,11},{14,12},{15,13},{16,18},{17,... | collective-permute-start | bytes 1572872 | tf_op jit(solution)/shard_map/ppermute | solution.py:47
  120.3 2.7 %collective-permute-done.18 = bf16[128,2048]{1,0:T(8,128)(2,1)S(1)} collective-permute-done((bf16[128,2048]{1,0:T(8,128)(2,1)S(1)}, bf16[128,2048]{1,0:T(8,128)(2,1)S(1)}, u32[]{:S(2)}, u32[]{:S(2)}) %collective-permute-start.18) | collective-permute-done | bytes 524320 | tf_op jit(solution)/shard_map/ppermute | solution.py:47
  126.6 7.0 %collective-permute-done.28 = bf16[128,2048]{1,0:T(8,128)(2,1)S(1)} collective-permute-done((bf16[128,2048]{1,0:T(8,128)(2,1)S(1)}, bf16[128,2048]{1,0:T(8,128)(2,1)S(1)}, u32[]{:S(2)}, u32[]{:S(2)}) %collective-permute-start.28) | collective-permute-done | bytes 524320 | tf_op jit(solution)/shard_map/ppermute | solution.py:47
  133.6 6.5 %collective-permute-done.27 = bf16[128,2048]{1,0:T(8,128)(2,1)S(1)} collective-permute-done((bf16[128,2048]{1,0:T(8,128)(2,1)S(1)}, bf16[128,2048]{1,0:T(8,128)(2,1)S(1)}, u32[]{:S(2)}, u32[]{:S(2)}) %collective-permute-start.27) | collective-permute-done | bytes 524320 | tf_op jit(solution)/shard_map/ppermute | solution.py:47
  140.5 2.0 %collective-permute-start.30 = (bf16[32,2048]{1,0:T(8,128)(2,1)S(1)}, bf16[32,2048]{1,0:T(8,128)(2,1)S(1)}, u32[]{:S(2)}, u32[]{:S(2)}) collective-permute-start(bf16[32,2048]{1,0:T(8,128)(2,1)S(1)} %get-tuple-element.148), channel_id=1, source_target_pairs={{0,8},{8,0},{16,24},{24,16},{1,9},{9,1},{17,25},{25,17},{2,10},{10... | collective-permute-start | bytes 393224 | tf_op jit(solution)/shard_map/ppermute | solution.py:489
  143.5 1.4 collective-permute-start.32
  145.0 1.8 %collective-permute-done.30.refs_1_ = bf16[32,2048]{1,0:T(8,128)(2,1)S(1)} collective-permute-done((bf16[32,2048]{1,0:T(8,128)(2,1)S(1)}, bf16[32,2048]{1,0:T(8,128)(2,1)S(1)}, u32[]{:S(2)}, u32[]{:S(2)}) %collective-permute-start.30) | collective-permute-done | bytes 131104 | tf_op jit(solution)/shard_map/ppermute | solution.py:489
  147.8 1.6 %collective-permute-done.32.refs_3_ = bf16[32,2048]{1,0:T(8,128)(2,1)S(1)} collective-permute-done((bf16[32,2048]{1,0:T(8,128)(2,1)S(1)}, bf16[32,2048]{1,0:T(8,128)(2,1)S(1)}, u32[]{:S(2)}, u32[]{:S(2)}) %collective-permute-start.32) | collective-permute-done | bytes 131104 | tf_op jit(solution)/shard_map/ppermute | solution.py:489
  (91 shorter events, 22.7 us)
Async XLA Ops:
  3.2 9.1 %collective-permute-start = (bf16[32,2048]{1,0:T(8,128)(2,1)}, bf16[32,2048]{1,0:T(8,128)(2,1)S(1)}, u32[]{:S(2)}, u32[]{:S(2)}) collective-permute-start(bf16[32,2048]{1,0:T(8,128)(2,1)} %get-tuple-element.74), channel_id=1, source_target_pairs={{0,8},{8,0},{16,24},{24,16},{1,9},{9,1},{17,25},{25,17},{2,10},{10... | collective-permute-start | bytes 393224 | tf_op jit(solution)/shard_map/ppermute | solution.py:489
  6.1 8.0 %collective-permute-start.1 = (bf16[32,2048]{1,0:T(8,128)(2,1)}, bf16[32,2048]{1,0:T(8,128)(2,1)S(1)}, u32[]{:S(2)}, u32[]{:S(2)}) collective-permute-start(bf16[32,2048]{1,0:T(8,128)(2,1)} %get-tuple-element.75), channel_id=1, source_target_pairs={{0,16},{8,24},{16,0},{24,8},{1,17},{9,25},{17,1},{25,9},{2,18},{10... | collective-permute-start | bytes 393224 | tf_op jit(solution)/shard_map/ppermute | solution.py:489
  7.7 6.5 %collective-permute-start.2 = (bf16[32,2048]{1,0:T(8,128)(2,1)}, bf16[32,2048]{1,0:T(8,128)(2,1)S(1)}, u32[]{:S(2)}, u32[]{:S(2)}) collective-permute-start(bf16[32,2048]{1,0:T(8,128)(2,1)} %get-tuple-element.76), channel_id=1, source_target_pairs={{0,24},{8,16},{16,8},{24,0},{1,25},{9,17},{17,9},{25,1},{2,26},{10... | collective-permute-start | bytes 393224 | tf_op jit(solution)/shard_map/ppermute | solution.py:489
  7.7 7.4 %collective-permute-start.3 = (bf16[256,128]{1,0:T(8,128)(2,1)}, bf16[256,128]{1,0:T(8,128)(2,1)S(1)}, u32[]{:S(2)}, u32[]{:S(2)}) collective-permute-start(bf16[256,128]{1,0:T(8,128)(2,1)} %get-tuple-element.82), channel_id=1, source_target_pairs={{0,8},{8,16},{16,24},{1,9},{9,17},{17,25},{2,10},{10,18},{18,26},{... | collective-permute-start | bytes 196616 | tf_op jit(solution)/shard_map/ppermute | solution.py:506
  23.6 16.9 %collective-permute-start.4 = (bf16[4,128,2048]{2,1,0:T(8,128)(2,1)}, bf16[4,128,2048]{2,1,0:T(8,128)(2,1)S(1)}, u32[]{:S(2)}, u32[]{:S(2)}) collective-permute-start(bf16[4,128,2048]{2,1,0:T(8,128)(2,1)} %attention.2), channel_id=1, source_target_pairs={{0,1},{1,0},{2,3},{3,2},{4,5},{5,4},{6,7},{7,6},{8,9},{9,8},{10,11... | collective-permute-start | bytes 6291464 | tf_op jit(solution)/shard_map/ppermute | solution.py:52
  23.6 14.3 %collective-permute-start.9 = (bf16[128,2048]{1,0:T(8,128)(2,1)S(1)}, bf16[128,2048]{1,0:T(8,128)(2,1)S(1)}, u32[]{:S(2)}, u32[]{:S(2)}) collective-permute-start(bf16[128,2048]{1,0:T(8,128)(2,1)S(1)} %pack.1.refs_0_), channel_id=1, source_target_pairs={{0,2},{1,3},{2,0},{3,1},{4,6},{5,7},{6,4},{7,5},{8,10},{9,11},{10,... | collective-permute-start | bytes 1572872 | tf_op jit(solution)/shard_map/ppermute | solution.py:47
  25.3 13.4 %collective-permute-start.12 = (bf16[128,2048]{1,0:T(8,128)(2,1)S(1)}, bf16[128,2048]{1,0:T(8,128)(2,1)S(1)}, u32[]{:S(2)}, u32[]{:S(2)}) collective-permute-start(bf16[128,2048]{1,0:T(8,128)(2,1)S(1)} %pack.1.refs_0_), channel_id=1, source_target_pairs={{2,4},{3,5},{4,2},{5,3},{10,12},{11,13},{12,10},{13,11},{18,20},{1... | collective-permute-start | bytes 1572872 | tf_op jit(solution)/shard_map/ppermute | solution.py:47
  38.0 15.3 %collective-permute-start.10 = (bf16[128,2048]{1,0:T(8,128)(2,1)S(1)}, bf16[128,2048]{1,0:T(8,128)(2,1)S(1)}, u32[]{:S(2)}, u32[]{:S(2)}) collective-permute-start(bf16[128,2048]{1,0:T(8,128)(2,1)S(1)} %collective-permute-done.9.refs_0_), channel_id=1, source_target_pairs={{2,4},{3,5},{4,2},{5,3},{10,12},{11,13},{12,10},{13,11},{18,20},{1... | collective-permute-start | bytes 1572872 | tf_op jit(solution)/shard_map/ppermute | solution.py:47
  38.7 17.0 %collective-permute-start.14 = (bf16[128,2048]{1,0:T(8,128)(2,1)S(1)}, bf16[128,2048]{1,0:T(8,128)(2,1)S(1)}, u32[]{:S(2)}, u32[]{:S(2)}) collective-permute-start(bf16[128,2048]{1,0:T(8,128)(2,1)S(1)} %collective-permute-done.12), channel_id=1, source_target_pairs={{2,0},{3,1},{4,6},{5,7},{10,8},{11,9},{12,14},{13,15},{18,16},{19,... | collective-permute-start | bytes 1572872 | tf_op jit(solution)/shard_map/ppermute | solution.py:47
  40.0 15.9 %collective-permute-start.6 = (bf16[128,2048]{1,0:T(8,128)(2,1)S(1)}, bf16[128,2048]{1,0:T(8,128)(2,1)S(1)}, u32[]{:S(2)}, u32[]{:S(2)}) collective-permute-start(bf16[128,2048]{1,0:T(8,128)(2,1)S(1)} %pack.1.refs_0_), channel_id=1, source_target_pairs={{0,1},{1,0},{2,3},{3,2},{4,5},{5,4},{6,7},{7,6},{8,9},{9,8},{10,11... | collective-permute-start | bytes 1572872 | tf_op jit(solution)/shard_map/ppermute | solution.py:52
  40.1 32.2 %collective-permute-start.16 = (bf16[128,2048]{1,0:T(8,128)(2,1)S(1)}, bf16[128,2048]{1,0:T(8,128)(2,1)S(1)}, u32[]{:S(2)}, u32[]{:S(2)}) collective-permute-start(bf16[128,2048]{1,0:T(8,128)(2,1)S(1)} %collective-permute-done.9.refs_0_), channel_id=1, source_target_pairs={{0,1},{1,0},{2,3},{3,2},{4,5},{5,4},{6,7},{7,6},{8,9},{9,8},{10,11... | collective-permute-start | bytes 1572872 | tf_op jit(solution)/shard_map/ppermute | solution.py:52
  46.9 22.8 %collective-permute-start.5 = (bf16[128,2048]{1,0:T(8,128)(2,1)S(1)}, bf16[128,2048]{1,0:T(8,128)(2,1)S(1)}, u32[]{:S(2)}, u32[]{:S(2)}) collective-permute-start(bf16[128,2048]{1,0:T(8,128)(2,1)S(1)} %get-tuple-element.111), channel_id=1, source_target_pairs={{0,2},{1,3},{6,4},{7,5},{8,10},{9,11},{14,12},{15,13},{16,18},{17,... | collective-permute-start | bytes 1572872 | tf_op jit(solution)/shard_map/ppermute | solution.py:47
  55.9 20.1 %collective-permute-start.15 = (bf16[128,2048]{1,0:T(8,128)(2,1)S(1)}, bf16[128,2048]{1,0:T(8,128)(2,1)S(1)}, u32[]{:S(2)}, u32[]{:S(2)}) collective-permute-start(bf16[128,2048]{1,0:T(8,128)(2,1)S(1)} %add_convert_fusion.9.refs_0_), channel_id=1, source_target_pairs={{0,1},{1,0},{2,3},{3,2},{4,5},{5,4},{6,7},{7,6},{8,9},{9,8},{10,11... | collective-permute-start | bytes 1572872 | tf_op jit(solution)/shard_map/ppermute | solution.py:52
  55.9 16.2 %collective-permute-start.11 = (bf16[128,2048]{1,0:T(8,128)(2,1)S(1)}, bf16[128,2048]{1,0:T(8,128)(2,1)S(1)}, u32[]{:S(2)}, u32[]{:S(2)}) collective-permute-start(bf16[128,2048]{1,0:T(8,128)(2,1)S(1)} %collective-permute-done.10), channel_id=1, source_target_pairs={{2,0},{3,1},{4,6},{5,7},{10,8},{11,9},{12,14},{13,15},{18,16},{19,... | collective-permute-start | bytes 1572872 | tf_op jit(solution)/shard_map/ppermute | solution.py:47
  57.2 26.4 %collective-permute-start.8 = (bf16[128,2048]{1,0:T(8,128)(2,1)S(1)}, bf16[128,2048]{1,0:T(8,128)(2,1)S(1)}, u32[]{:S(2)}, u32[]{:S(2)}) collective-permute-start(bf16[128,2048]{1,0:T(8,128)(2,1)S(1)} %get-tuple-element.98), channel_id=1, source_target_pairs={{0,2},{1,3},{6,4},{7,5},{8,10},{9,11},{14,12},{15,13},{16,18},{17,... | collective-permute-start | bytes 1572872 | tf_op jit(solution)/shard_map/ppermute | solution.py:47
  69.9 14.3 %collective-permute-start.7 = (bf16[128,2048]{1,0:T(8,128)(2,1)S(1)}, bf16[128,2048]{1,0:T(8,128)(2,1)S(1)}, u32[]{:S(2)}, u32[]{:S(2)}) collective-permute-start(bf16[128,2048]{1,0:T(8,128)(2,1)S(1)} %add_convert_fusion.11), channel_id=1, source_target_pairs={{4,2},{5,3},{2,4},{3,5},{12,10},{13,11},{10,12},{11,13},{20,18},{2... | collective-permute-start | bytes 1572872 | tf_op jit(solution)/shard_map/ppermute | solution.py:47
  72.3 7.8 %collective-permute-start.13 = (bf16[128,2048]{1,0:T(8,128)(2,1)S(1)}, bf16[128,2048]{1,0:T(8,128)(2,1)S(1)}, u32[]{:S(2)}, u32[]{:S(2)}) collective-permute-start(bf16[128,2048]{1,0:T(8,128)(2,1)S(1)} %add_convert_fusion.10.refs_0_), channel_id=1, source_target_pairs={{0,1},{1,0},{2,3},{3,2},{4,5},{5,4},{6,7},{7,6},{8,9},{9,8},{10,11... | collective-permute-start | bytes 1572872 | tf_op jit(solution)/shard_map/ppermute | solution.py:52
  79.5 8.8 %collective-permute-start.21 = (bf16[128,2048]{1,0:T(8,128)(2,1)S(1)}, bf16[128,2048]{1,0:T(8,128)(2,1)S(1)}, u32[]{:S(2)}, u32[]{:S(2)}) collective-permute-start(bf16[128,2048]{1,0:T(8,128)(2,1)S(1)} %get-tuple-element.117), channel_id=1, source_target_pairs={{0,1},{1,0},{2,3},{3,2},{4,5},{5,4},{6,7},{7,6},{8,9},{9,8},{10,11... | collective-permute-start | bytes 1572872 | tf_op jit(solution)/shard_map/ppermute | solution.py:52
  80.0 9.7 %collective-permute-start.20 = (bf16[128,2048]{1,0:T(8,128)(2,1)S(1)}, bf16[128,2048]{1,0:T(8,128)(2,1)S(1)}, u32[]{:S(2)}, u32[]{:S(2)}) collective-permute-start(bf16[128,2048]{1,0:T(8,128)(2,1)S(1)} %get-tuple-element.116), channel_id=1, source_target_pairs={{0,1},{1,0},{2,3},{3,2},{4,5},{5,4},{6,7},{7,6},{8,9},{9,8},{10,11... | collective-permute-start | bytes 1572872 | tf_op jit(solution)/shard_map/ppermute | solution.py:52
  85.8 14.7 %collective-permute-start.23 = (bf16[128,2048]{1,0:T(8,128)(2,1)S(1)}, bf16[128,2048]{1,0:T(8,128)(2,1)S(1)}, u32[]{:S(2)}, u32[]{:S(2)}) collective-permute-start(bf16[128,2048]{1,0:T(8,128)(2,1)S(1)} %add_convert_fusion.6), channel_id=1, source_target_pairs={{0,2},{1,3},{6,4},{7,5},{8,10},{9,11},{14,12},{15,13},{16,18},{17,... | collective-permute-start | bytes 1572872 | tf_op jit(solution)/shard_map/ppermute | solution.py:47
  88.4 23.4 %collective-permute-start.25 = (bf16[128,2048]{1,0:T(8,128)(2,1)S(1)}, bf16[128,2048]{1,0:T(8,128)(2,1)S(1)}, u32[]{:S(2)}, u32[]{:S(2)}) collective-permute-start(bf16[128,2048]{1,0:T(8,128)(2,1)S(1)} %add_convert_fusion.5), channel_id=1, source_target_pairs={{0,2},{1,3},{6,4},{7,5},{8,10},{9,11},{14,12},{15,13},{16,18},{17,... | collective-permute-start | bytes 1572872 | tf_op jit(solution)/shard_map/ppermute | solution.py:47
  100.8 11.9 %collective-permute-start.24 = (bf16[128,2048]{1,0:T(8,128)(2,1)S(1)}, bf16[128,2048]{1,0:T(8,128)(2,1)S(1)}, u32[]{:S(2)}, u32[]{:S(2)}) collective-permute-start(bf16[128,2048]{1,0:T(8,128)(2,1)S(1)} %add_convert_fusion.3), channel_id=1, source_target_pairs={{4,2},{5,3},{2,4},{3,5},{12,10},{13,11},{10,12},{11,13},{20,18},{2... | collective-permute-start | bytes 1572872 | tf_op jit(solution)/shard_map/ppermute | solution.py:47
  101.5 21.5 %collective-permute-start.18 = (bf16[128,2048]{1,0:T(8,128)(2,1)S(1)}, bf16[128,2048]{1,0:T(8,128)(2,1)S(1)}, u32[]{:S(2)}, u32[]{:S(2)}) collective-permute-start(bf16[128,2048]{1,0:T(8,128)(2,1)S(1)} %get-tuple-element.115), channel_id=1, source_target_pairs={{0,2},{1,3},{6,4},{7,5},{8,10},{9,11},{14,12},{15,13},{16,18},{17,... | collective-permute-start | bytes 1572872 | tf_op jit(solution)/shard_map/ppermute | solution.py:47
  107.9 18.7 %collective-permute-start.26 = (bf16[128,2048]{1,0:T(8,128)(2,1)S(1)}, bf16[128,2048]{1,0:T(8,128)(2,1)S(1)}, u32[]{:S(2)}, u32[]{:S(2)}) collective-permute-start(bf16[128,2048]{1,0:T(8,128)(2,1)S(1)} %get-tuple-element.138), channel_id=1, source_target_pairs={{0,1},{1,0},{2,3},{3,2},{4,5},{5,4},{6,7},{7,6},{8,9},{9,8},{10,11... | collective-permute-start | bytes 1572872 | tf_op jit(solution)/shard_map/ppermute | solution.py:52
  108.0 16.2 %collective-permute-start.17 = (bf16[128,2048]{1,0:T(8,128)(2,1)S(1)}, bf16[128,2048]{1,0:T(8,128)(2,1)S(1)}, u32[]{:S(2)}, u32[]{:S(2)}) collective-permute-start(bf16[128,2048]{1,0:T(8,128)(2,1)S(1)} %add_convert_fusion.7), channel_id=1, source_target_pairs={{2,0},{3,1},{4,6},{5,7},{10,8},{11,9},{12,14},{13,15},{18,16},{19,... | collective-permute-start | bytes 1572872 | tf_op jit(solution)/shard_map/ppermute | solution.py:47
  111.8 13.7 %collective-permute-start.19 = (bf16[128,2048]{1,0:T(8,128)(2,1)S(1)}, bf16[128,2048]{1,0:T(8,128)(2,1)S(1)}, u32[]{:S(2)}, u32[]{:S(2)}) collective-permute-start(bf16[128,2048]{1,0:T(8,128)(2,1)S(1)} %add_convert_fusion.8), channel_id=1, source_target_pairs={{4,2},{5,3},{2,4},{3,5},{12,10},{13,11},{10,12},{11,13},{20,18},{2... | collective-permute-start | bytes 1572872 | tf_op jit(solution)/shard_map/ppermute | solution.py:47
  112.7 20.9 %collective-permute-start.28 = (bf16[128,2048]{1,0:T(8,128)(2,1)S(1)}, bf16[128,2048]{1,0:T(8,128)(2,1)S(1)}, u32[]{:S(2)}, u32[]{:S(2)}) collective-permute-start(bf16[128,2048]{1,0:T(8,128)(2,1)S(1)} %add_convert_fusion.4), channel_id=1, source_target_pairs={{0,2},{1,3},{6,4},{7,5},{8,10},{9,11},{14,12},{15,13},{16,18},{17,... | collective-permute-start | bytes 1572872 | tf_op jit(solution)/shard_map/ppermute | solution.py:47
  123.0 10.6 %collective-permute-start.29 = (bf16[128,2048]{1,0:T(8,128)(2,1)S(1)}, bf16[128,2048]{1,0:T(8,128)(2,1)S(1)}, u32[]{:S(2)}, u32[]{:S(2)}) collective-permute-start(bf16[128,2048]{1,0:T(8,128)(2,1)S(1)} %add_convert_fusion.2), channel_id=1, source_target_pairs={{4,2},{5,3},{2,4},{3,5},{12,10},{13,11},{10,12},{11,13},{20,18},{2... | collective-permute-start | bytes 1572872 | tf_op jit(solution)/shard_map/ppermute | solution.py:47
  124.2 16.0 %collective-permute-start.27 = (bf16[128,2048]{1,0:T(8,128)(2,1)S(1)}, bf16[128,2048]{1,0:T(8,128)(2,1)S(1)}, u32[]{:S(2)}, u32[]{:S(2)}) collective-permute-start(bf16[128,2048]{1,0:T(8,128)(2,1)S(1)} %add_convert_fusion.1), channel_id=1, source_target_pairs={{2,0},{3,1},{4,6},{5,7},{10,8},{11,9},{12,14},{13,15},{18,16},{19,... | collective-permute-start | bytes 1572872 | tf_op jit(solution)/shard_map/ppermute | solution.py:47
  140.5 6.3 %collective-permute-start.30 = (bf16[32,2048]{1,0:T(8,128)(2,1)S(1)}, bf16[32,2048]{1,0:T(8,128)(2,1)S(1)}, u32[]{:S(2)}, u32[]{:S(2)}) collective-permute-start(bf16[32,2048]{1,0:T(8,128)(2,1)S(1)} %get-tuple-element.148), channel_id=1, source_target_pairs={{0,8},{8,0},{16,24},{24,16},{1,9},{9,1},{17,25},{25,17},{2,10},{10... | collective-permute-start | bytes 393224 | tf_op jit(solution)/shard_map/ppermute | solution.py:489
  142.4 5.3 %collective-permute-start.31 = (bf16[32,2048]{1,0:T(8,128)(2,1)S(1)}, bf16[32,2048]{1,0:T(8,128)(2,1)S(1)}, u32[]{:S(2)}, u32[]{:S(2)}) collective-permute-start(bf16[32,2048]{1,0:T(8,128)(2,1)S(1)} %get-tuple-element.147), channel_id=1, source_target_pairs={{0,16},{8,24},{16,0},{24,8},{1,17},{9,25},{17,1},{25,9},{2,18},{10... | collective-permute-start | bytes 393224 | tf_op jit(solution)/shard_map/ppermute | solution.py:489
  143.5 5.9 %collective-permute-start.32 = (bf16[32,2048]{1,0:T(8,128)(2,1)S(1)}, bf16[32,2048]{1,0:T(8,128)(2,1)S(1)}, u32[]{:S(2)}, u32[]{:S(2)}) collective-permute-start(bf16[32,2048]{1,0:T(8,128)(2,1)S(1)} %get-tuple-element.146), channel_id=1, source_target_pairs={{0,24},{8,16},{16,8},{24,0},{1,25},{9,17},{17,9},{25,1},{2,26},{10... | collective-permute-start | bytes 393224 | tf_op jit(solution)/shard_map/ppermute | solution.py:489
  (17 other events, 392.4 us)

commit v2 on v1

--- a/solution.py
+++ b/solution.py
@@ -109,7 +109,7 @@
         return [v for v in values if v is not None]
 
     def step(self, s, slots):
-        for parity in (1, 0):
+        for parity in (0, 1):
             pairs = scatter_pairs(self.n, s, parity)
             if pairs:
                 slot = slots[self.n - s] if parity == 0 else slots[s]
@@ -142,12 +142,26 @@
     return group, rank, slot, slot_col
 
 
-def dispatch_kernel(
-    capacity, block, me_ref, x_ref, gain_ref, ids_ref, share_ref, k_ref, v_ref, *out_refs
-):
-    *out_refs, tail_ref = out_refs
+def tails_kernel(k_ref, v_ref, tail_ref):
     tail_ref[:WINDOW] = k_ref[...]
     tail_ref[WINDOW:] = v_ref[...]
+
+
+def last_rows(keys, values):
+    rows, narrow = keys.shape
+    last = pl.BlockSpec((WINDOW, narrow), lambda i: (rows // WINDOW - 1, 0))
+    return pl.pallas_call(
+        tails_kernel,
+        grid=(1,),
+        in_specs=[last, last],
+        out_specs=pl.BlockSpec((2 * WINDOW, narrow), lambda i: (0, 0)),
+        out_shape=jax.ShapeDtypeStruct((2 * WINDOW, narrow), BF),
+        compiler_params=pltpu.CompilerParams(vmem_limit_bytes=60 << 20),
+        name="last_rows",
+    )(keys, values)
+
+
+def dispatch_kernel(capacity, block, me_ref, x_ref, gain_ref, ids_ref, share_ref, *out_refs):
     rows = len(out_refs) * block
     tokens = x_ref.shape[0]
     lanes = 128
@@ -178,26 +192,23 @@
     return [pl.BlockSpec(memory_space=pltpu.VMEM)] * count
 
 
-def dispatch(me, x, gain, ids, share, keys, values, n_groups, capacity, block):
-    rows, narrow = keys.shape
+def dispatch(me, x, gain, ids, share, n_groups, capacity, block):
     gain = gain.reshape(1, -1)
-    last = pl.BlockSpec((WINDOW, narrow), lambda i: (rows // WINDOW - 1, 0))
 
     def whole(shape):
         return pl.BlockSpec(shape, lambda i: (0, 0))
 
-    outs = [(block, x.shape[1])] * n_groups + [(2 * WINDOW, narrow)]
+    outs = [(block, x.shape[1])] * n_groups
     return pl.pallas_call(
         functools.partial(dispatch_kernel, capacity, block),
         grid=(1,),
         in_specs=[pl.BlockSpec(memory_space=pltpu.SMEM)]
-        + [whole(v.shape) for v in (x, gain, ids, share)]
-        + [last, last],
+        + [whole(v.shape) for v in (x, gain, ids, share)],
         out_specs=[whole(o) for o in outs],
         out_shape=[jax.ShapeDtypeStruct(o, BF) for o in outs],
         compiler_params=pltpu.CompilerParams(vmem_limit_bytes=60 << 20),
         name="dispatch",
-    )(me, x, gain, ids, share, keys, values)
+    )(me, x, gain, ids, share)
 
 
 def pack_kernel(*refs):
@@ -449,7 +460,7 @@
         ),
         out_shape=out_shape,
         cost_estimate=pl.CostEstimate(
-            flops=2 * count * WINDOW * width * (weight.shape[1] + 4 * WINDOW),
+            flops=16 * count * WINDOW * width * (weight.shape[1] + 4 * WINDOW),
             bytes_accessed=2 * weight.size + 2 * count * WINDOW * (weight.shape[1] + 2 * width),
             transcendentals=count * WINDOW * 2 * WINDOW * kv_here * per_group,
         ),
@@ -488,22 +499,13 @@
     def around(part, k):
         return lax.ppermute(part, "ep", [(i, i ^ k) for i in range(n_groups)])
 
-    *send, tails = dispatch(
-        me,
-        expert_input,
-        norm_gain,
-        ids,
-        route_weight.T,
-        key_rows,
-        value_rows,
-        n_groups,
-        capacity,
-        block,
-    )
+    tails = seq.did(last_rows(key_rows, value_rows))
+    before = lax.ppermute(tails, "ep", [(i, i + 1) for i in range(n_groups - 1)])
+    (x,) = seq.after(expert_input)
+    send = dispatch(me, x, norm_gain, ids, route_weight.T, n_groups, capacity, block)
     seq.did(send[0])
     got = [send[0]] + [around(send[k], k) for k in range(1, n_groups)]
 
-    before = lax.ppermute(tails, "ep", [(i, i + 1) for i in range(n_groups - 1)])
     chunk = jnp.stack([slot_chunk(n, z, k) for k in range(n)]) * CORES
 
     def attend(order, plus=None):
@@ -551,45 +553,53 @@
             seq.did(done[0])
             back[k] = [done[0], core_swap(done[1])]
 
+    other = seq.did(attend(chunk + 1 - core))
+    swapped = core_swap(other)
+    weights = seq.after(gate_weight, up_weight, down_weight.reshape(-1, width))
     own = seq.did(pack(seq.after(*got)))
     gather(1)
     slots[0] = [own, core_swap(own)]
-    other = seq.did(attend(chunk + 1 - core))
-    swapped = core_swap(other)
-    weights = seq.after(gate_weight, up_weight, down_weight.reshape(-1, width))
+    (swapped,) = seq.after(swapped)
+    mine = attend(chunk + core, swapped)
+    seq.did(mine[0])
+    attn = [[v] for v in mine]
     attn_scatter = LineScatter(n, seq)
     for s in range(1, n):
-        todo = [k for k in slots if k not in back]
-        if s == n - 1:
-            experts(todo)
-        else:
+        if s < n - 1:
             gather(s + 1)
         prepare(s)
         if s == 1:
-            (swapped,) = seq.after(swapped)
-            mine = attend(chunk + core, swapped)
-            seq.did(mine[0])
-            attn = [[v] for v in mine]
             for a in range(1, n):
                 attn_scatter.start(a, attn[n - a])
         elif s < n - 1:
-            experts(todo[:1])
             attn_scatter.step(s, attn)
-            experts(todo[1:])
-    experts([k for k in slots if k not in back])
+        experts([k for k in slots if k not in back])
     attn_scatter.step(n - 1, attn)
 
-    scatter = LineScatter(n, seq)
+    half = n_groups * block // 2
+    lines = []
+    for h in range(2):
+        part = slice(h * half, (h + 1) * half)
+        pieces = [[(v, part) for v in back[k]] for k in range(n)]
+        lines.append((LineScatter(n, seq), pieces))
     for s in range(1, n):
-        scatter.start(s, back[n - s])
+        for scatter, pieces in lines:
+            scatter.start(s, pieces[n - s])
     for s in range(2, n):
-        scatter.step(s, back)
+        for scatter, pieces in lines:
+            scatter.step(s, pieces)
     attn_output = seq.did(add_all(seq.after(*attn_scatter.finish(attn[0]))))
-    addends = seq.after(*scatter.finish(back[0]))
     home = []
-    for k in range(n_groups):
-        part = add_all([v[k * block : (k + 1) * block] for v in addends])
-        home.append(around(part, k) if k else part)
+    for h, (scatter, pieces) in enumerate(lines):
+        addends = seq.after(*scatter.finish(pieces[0]))
+        for k in range(n_groups // 2):
+            values = []
+            for v in addends:
+                v, first = (v[0], v[1].start) if isinstance(v, tuple) else (v, 0)
+                values.append((v, slice(first + k * block, first + (k + 1) * block)))
+            part = seq.did(add_all(values))
+            k += h * n_groups // 2
+            home.append(around(part, k) if k else part)
     expert_output = combine(me, ids, home)
     return (attn_output, expert_output)
 

time: 151 us -> 185 us (1.23)
  starting transfers between devices: 54.2 us -> 83.4 us
  waiting for transfers between devices: 53.2 us -> 60.2 us
  local copies, waits for them, and re-layouts: 6.8 us -> 1.55 us
    ppermute x17 -> x23, starting transfers between devices: 39.6 us -> 70.6 us  [along(): return lax.ppermute(value, 'tp', full)]
    unnamed x32 -> x36, local copies, waits for them, and re-layouts: 6.8 us -> 1.55 us
    ppermute x6, waiting for transfers between devices: 6.25 us -> 11.1 us  [around(): return lax.ppermute(part, 'ep', [(i, i ^ k) for i in range(n_groups)])]
    ppermute x17 -> x23, waiting for transfers between devices: 45.6 us -> 48.8 us  [along(): return lax.ppermute(value, 'tp', full)]
    ppermute x6, starting transfers between devices: 8.92 us -> 6.62 us  [around(): return lax.ppermute(part, 'ep', [(i, i ^ k) for i in range(n_groups)])]
  transfers between devices with their start and end apart: 33 -> 39, of which waited for: 14 -> 15; matrix products, arithmetic and copies ran while one was open for 2% -> 2% of each run, Pallas kernels for 13% -> 12%
where the time goes in v2:
time: 185 us; the launch traced here: 183 us
  starting transfers between devices  83.4 us (45%)
  waiting for transfers between devices  60.2 us (33%)
  Pallas kernels  32.6 us (18%)
  other arithmetic  3.68 us (2%)
    ppermute x23, starting transfers between devices, along(): return lax.ppermute(value, 'tp', full)  70.6 us
    ppermute x23, waiting for transfers between devices, along(): return lax.ppermute(value, 'tp', full)  48.8 us
    pallas_call x4, Pallas kernels, expert_rows(): pl.pallas_call(functools.partial(expert_kernel, capacity, block, count),...  14.1 us
    pallas_call x2, Pallas kernels, attention_partials(): pl.pallas_call(functools.partial(attention_kernel, kv_here, per_group, ma...  13.6 us
    ppermute x6, waiting for transfers between devices, around(): return lax.ppermute(part, 'ep', [(i, i ^ k) for i in range(n_groups)])  11.1 us
    ppermute x6, starting transfers between devices, around(): return lax.ppermute(part, 'ep', [(i, i ^ k) for i in range(n_groups)])  6.62 us
    ppermute x1, starting transfers between devices, body(): lax.ppermute(tails, 'ep', [(i, i + 1) for i in range(n_groups - 1)])  4.86 us
  transfers between devices with their start and end apart: 39, of which 15 were waited for; matrix products, arithmetic and copies ran while one was open for 2% of the time, Pallas kernels for 12%

profile of v2, /device:TPU:0, one launch (start us, length us, event | category | flops | bytes accessed | tf_op | source)
XLA Modules:
  0.0 182.9 jit_solution(17755304838806183281)
XLA Ops:
  2.0 4.9 %collective-permute-start.3 = (bf16[256,128]{1,0:T(8,128)(2,1)}, bf16[256,128]{1,0:T(8,128)(2,1)S(1)}, u32[]{:S(2)}, u32[]{:S(2)}) collective-permute-start(bf16[256,128]{1,0:T(8,128)(2,1)} %last_rows.1), channel_id=1, source_target_pairs={{0,8},{8,16},{16,24},{1,9},{9,17},{17,25},{2,10},{10,18},{18,26},{... | collective-permute-start | bytes 196616 | tf_op jit(solution)/shard_map/ppermute | solution.py:503
  7.0 2.3 %dispatch.1 = (bf16[32,2048]{1,0:T(8,128)(2,1)}, bf16[32,2048]{1,0:T(8,128)(2,1)}, bf16[32,2048]{1,0:T(8,128)(2,1)}, bf16[32,2048]{1,0:T(8,128)(2,1)}) custom-call(s32[1]{0:T(128)} %bitcast.5.me_ref, bf16[96,2048]{1,0:T(8,128)(2,1)} %x_ref, f32[1,2048]{1,0:T(1,128)} %bitcast.16, s32[1,96]{1,0:T(1,128)} %bitcast.14, f32[2,96]{1,0:T(2,128)} %bitcast.17), custom_call_target="tpu_custom_call" | custom-call | tf_op jit(solution)/shard_map/dispatch/pallas_call | solution.py:202
  10.6 8.1 %attention.2 = bf16[4,128,2048]{2,1,0:T(8,128)(2,1)} custom-call(s32[4]{0:T(128)} %get-tuple-element.184.order_ref, s32[1]{0:T(128)} %bitcast.4.base_ref, f32[4]{0:T(128)} %sink_ref.3, bf16[1024,256]{1,0:T(8,128)(2,1)} %q_ref.1, bf16[1024,128]{1,0:T(8,128)(2,1)} %k_ref.5, bf16[1024,128]{1,0:T(8,128)(2,1)} %v_ref.5, bf16[256,128]{1,0:T(8,128)(2,1)} %copy-done.9, ...), custom_call_target="tpu_custom_call" | custom-call | flops 5368709120 | bytes 3670016 | tf_op jit(solution)/shard_map/attention/pallas_call | solution.py:453
  18.7 1.6 collective-permute-start
  20.3 1.5 collective-permute-start.1
  22.8 2.2 %collective-permute-done.refs_1_ = bf16[32,2048]{1,0:T(8,128)(2,1)S(1)} collective-permute-done((bf16[32,2048]{1,0:T(8,128)(2,1)S(1)}, bf16[32,2048]{1,0:T(8,128)(2,1)S(1)}, u32[]{:S(2)}, u32[]{:S(2)}) %collective-permute-start) | collective-permute-done | bytes 131104 | tf_op jit(solution)/shard_map/ppermute | solution.py:500
  25.0 2.8 %collective-permute-done.1.refs_2_ = bf16[32,2048]{1,0:T(8,128)(2,1)S(1)} collective-permute-done((bf16[32,2048]{1,0:T(8,128)(2,1)S(1)}, bf16[32,2048]{1,0:T(8,128)(2,1)S(1)}, u32[]{:S(2)}, u32[]{:S(2)}) %collective-permute-start.1) | collective-permute-done | bytes 131104 | tf_op jit(solution)/shard_map/ppermute | solution.py:500
  27.7 1.6 collective-permute-done.2.refs_3_
  29.3 1.6 collective-permute-start.6
  31.7 11.1 %collective-permute-done.6.refs_0_ = bf16[128,2048]{1,0:T(8,128)(2,1)S(1)} collective-permute-done((bf16[128,2048]{1,0:T(8,128)(2,1)S(1)}, bf16[128,2048]{1,0:T(8,128)(2,1)S(1)}, u32[]{:S(2)}, u32[]{:S(2)}) %collective-permute-start.6) | collective-permute-done | bytes 524320 | tf_op jit(solution)/shard_map/ppermute | solution.py:47
  43.7 5.5 %attention.3 = (bf16[128,2048]{1,0:T(8,128)(2,1)S(1)}, bf16[128,2048]{1,0:T(8,128)(2,1)S(1)}, bf16[128,2048]{1,0:T(8,128)(2,1)S(1)}, bf16[128,2048]{1,0:T(8,128)(2,1)S(1)}) custom-call(s32[4]{0:T(128)S(1)} %broadcast_add_fusion.order_ref, s32[1]{0:T(128)} %bitcast.4.base_ref, f32[4]{0:T(128)S(1)} %copy-done.11, bf16[1024,256]{1,0:T(8,128)(2,1)S(1)} %copy-done.8, ...), custom_call_target="tpu_custom_call" | custom-call | flops 5368709120 | bytes 3670016 | tf_op jit(solution)/shard_map/attention/pallas_call | solution.py:453
  49.3 3.5 %collective-permute-start.5 = (bf16[128,2048]{1,0:T(8,128)(2,1)S(1)}, bf16[128,2048]{1,0:T(8,128)(2,1)S(1)}, u32[]{:S(2)}, u32[]{:S(2)}) collective-permute-start(bf16[128,2048]{1,0:T(8,128)(2,1)S(1)} %get-tuple-element.134), channel_id=1, source_target_pairs={{0,2},{1,3},{6,4},{7,5},{8,10},{9,11},{14,12},{15,13},{16,18},{17,... | collective-permute-start | bytes 1572872 | tf_op jit(solution)/shard_map/ppermute | solution.py:47
  54.8 3.5 %experts.4 = (bf16[128,2048]{1,0:T(8,128)(2,1)S(1)}, bf16[128,2048]{1,0:T(8,128)(2,1)S(1)}) custom-call(bf16[128,2048]{1,0:T(8,128)(2,1)S(1)} %pack.1.refs_0_, bf16[128,2048]{1,0:T(8,128)(2,1)S(1)} %collective-permute-done.8.refs_1_, bf16[2,2048,512]{2,1,0:T(8,128)(2,1)S(1)} %copy-done, bf16[2,2048,512]{2,1,0:T(8,128)(2,1)S(1)} %copy-done.1, ...), custom_call_target="tpu_custom_call" | custom-call | flops 3221225472 | bytes 2097152 | tf_op jit(solution)/shard_map/experts/pallas_call | solution.py:292
  58.4 3.5 %experts.5 = (bf16[128,2048]{1,0:T(8,128)(2,1)S(1)}, bf16[128,2048]{1,0:T(8,128)(2,1)S(1)}) custom-call(bf16[128,2048]{1,0:T(8,128)(2,1)S(1)} %collective-permute-done.6.refs_0_, bf16[128,2048]{1,0:T(8,128)(2,1)S(1)} %collective-permute-done.7.refs_1_, bf16[2,2048,512]{2,1,0:T(8,128)(2,1)S(1)} %copy-done, bf16[2,2048,512]{2,1,0:T(8,128)(2,1)S(1)} %copy-done.1, ...), custom_call_target="tpu_custom_call" | custom-call | flops 3221225472 | bytes 2097152 | tf_op jit(solution)/shard_map/experts/pallas_call | solution.py:292
  63.2 8.4 %collective-permute-start.17 = (bf16[128,2048]{1,0:T(8,128)(2,1)S(1)}, bf16[128,2048]{1,0:T(8,128)(2,1)S(1)}, u32[]{:S(2)}, u32[]{:S(2)}) collective-permute-start(bf16[128,2048]{1,0:T(8,128)(2,1)S(1)} %get-tuple-element.132), channel_id=1, source_target_pairs={{0,2},{1,3},{6,4},{7,5},{8,10},{9,11},{14,12},{15,13},{16,18},{17,... | collective-permute-start | bytes 1572872 | tf_op jit(solution)/shard_map/ppermute | solution.py:47
  71.6 1.5 collective-permute-start.18
  73.9 7.4 %collective-permute-done.11 = bf16[128,2048]{1,0:T(8,128)(2,1)S(1)} collective-permute-done((bf16[128,2048]{1,0:T(8,128)(2,1)S(1)}, bf16[128,2048]{1,0:T(8,128)(2,1)S(1)}, u32[]{:S(2)}, u32[]{:S(2)}) %collective-permute-start.11) | collective-permute-done | bytes 524320 | tf_op jit(solution)/shard_map/ppermute | solution.py:47
  82.4 3.5 %experts.6 = (bf16[128,2048]{1,0:T(8,128)(2,1)S(1)}, bf16[128,2048]{1,0:T(8,128)(2,1)S(1)}) custom-call(bf16[128,2048]{1,0:T(8,128)(2,1)S(1)} %add_convert_fusion.3.refs_0_, bf16[128,2048]{1,0:T(8,128)(2,1)S(1)} %collective-permute-done.15.refs_1_, bf16[2,2048,512]{2,1,0:T(8,128)(2,1)S(1)} %copy-done, bf16[2,2048,512]{2,1,0:T(8,128)(2,1)S(1)} %copy-done.1, ...), custom_call_target="tpu_custom_call" | custom-call | flops 3221225472 | bytes 2097152 | tf_op jit(solution)/shard_map/experts/pallas_call | solution.py:292
  86.5 3.5 %experts.7 = (bf16[128,2048]{1,0:T(8,128)(2,1)S(1)}, bf16[128,2048]{1,0:T(8,128)(2,1)S(1)}) custom-call(bf16[128,2048]{1,0:T(8,128)(2,1)S(1)} %add_convert_fusion.4.refs_0_, bf16[128,2048]{1,0:T(8,128)(2,1)S(1)} %collective-permute-done.13.refs_1_, bf16[2,2048,512]{2,1,0:T(8,128)(2,1)S(1)} %copy-done, bf16[2,2048,512]{2,1,0:T(8,128)(2,1)S(1)} %copy-done.1, ...), custom_call_target="tpu_custom_call" | custom-call | flops 3221225472 | bytes 2097152 | tf_op jit(solution)/shard_map/experts/pallas_call | solution.py:292
  90.3 3.5 %collective-permute-done.18 = bf16[128,2048]{1,0:T(8,128)(2,1)S(1)} collective-permute-done((bf16[128,2048]{1,0:T(8,128)(2,1)S(1)}, bf16[128,2048]{1,0:T(8,128)(2,1)S(1)}, u32[]{:S(2)}, u32[]{:S(2)}) %collective-permute-start.18) | collective-permute-done | bytes 524320 | tf_op jit(solution)/shard_map/ppermute | solution.py:47
  96.6 9.9 %collective-permute-start.25 = (bf16[64,2048]{1,0:T(8,128)(2,1)S(1)}, bf16[64,2048]{1,0:T(8,128)(2,1)S(1)}, u32[]{:S(2)}, u32[]{:S(2)}) collective-permute-start(bf16[64,2048]{1,0:T(8,128)(2,1)S(1)} %add_convert_fusion.17), channel_id=1, source_target_pairs={{0,2},{1,3},{6,4},{7,5},{8,10},{9,11},{14,12},{15,13},{16,18},{17,... | collective-permute-start | bytes 786440 | tf_op jit(solution)/shard_map/ppermute | solution.py:47
  106.6 5.4 %collective-permute-done.25 = bf16[64,2048]{1,0:T(8,128)(2,1)S(1)} collective-permute-done((bf16[64,2048]{1,0:T(8,128)(2,1)S(1)}, bf16[64,2048]{1,0:T(8,128)(2,1)S(1)}, u32[]{:S(2)}, u32[]{:S(2)}) %collective-permute-start.25) | collective-permute-done | bytes 262176 | tf_op jit(solution)/shard_map/ppermute | solution.py:47
  112.0 4.4 %collective-permute-start.24 = (bf16[64,2048]{1,0:T(8,128)(2,1)S(1)}, bf16[64,2048]{1,0:T(8,128)(2,1)S(1)}, u32[]{:S(2)}, u32[]{:S(2)}) collective-permute-start(bf16[64,2048]{1,0:T(8,128)(2,1)S(1)} %add_convert_fusion.16), channel_id=1, source_target_pairs={{0,2},{1,3},{6,4},{7,5},{8,10},{9,11},{14,12},{15,13},{16,18},{17,... | collective-permute-start | bytes 786440 | tf_op jit(solution)/shard_map/ppermute | solution.py:47
  116.5 4.6 %collective-permute-done.24 = bf16[64,2048]{1,0:T(8,128)(2,1)S(1)} collective-permute-done((bf16[64,2048]{1,0:T(8,128)(2,1)S(1)}, bf16[64,2048]{1,0:T(8,128)(2,1)S(1)}, u32[]{:S(2)}, u32[]{:S(2)}) %collective-permute-start.24) | collective-permute-done | bytes 262176 | tf_op jit(solution)/shard_map/ppermute | solution.py:47
  121.9 11.9 %collective-permute-start.27 = (bf16[64,2048]{1,0:T(8,128)(2,1)S(1)}, bf16[64,2048]{1,0:T(8,128)(2,1)S(1)}, u32[]{:S(2)}, u32[]{:S(2)}) collective-permute-start(bf16[64,2048]{1,0:T(8,128)(2,1)S(1)} %add_convert_fusion.15), channel_id=1, source_target_pairs={{0,2},{1,3},{6,4},{7,5},{8,10},{9,11},{14,12},{15,13},{16,18},{17,... | collective-permute-start | bytes 786440 | tf_op jit(solution)/shard_map/ppermute | solution.py:47
  133.8 3.8 %collective-permute-done.27 = bf16[64,2048]{1,0:T(8,128)(2,1)S(1)} collective-permute-done((bf16[64,2048]{1,0:T(8,128)(2,1)S(1)}, bf16[64,2048]{1,0:T(8,128)(2,1)S(1)}, u32[]{:S(2)}, u32[]{:S(2)}) %collective-permute-start.27) | collective-permute-done | bytes 262176 | tf_op jit(solution)/shard_map/ppermute | solution.py:47
  138.4 11.8 %collective-permute-start.22 = (bf16[64,2048]{1,0:T(8,128)(2,1)S(1)}, bf16[64,2048]{1,0:T(8,128)(2,1)S(1)}, u32[]{:S(2)}, u32[]{:S(2)}) collective-permute-start(bf16[64,2048]{1,0:T(8,128)(2,1)S(1)} %add_convert_fusion.14), channel_id=1, source_target_pairs={{0,2},{1,3},{6,4},{7,5},{8,10},{9,11},{14,12},{15,13},{16,18},{17,... | collective-permute-start | bytes 786440 | tf_op jit(solution)/shard_map/ppermute | solution.py:47
  150.4 5.7 %collective-permute-done.22 = bf16[64,2048]{1,0:T(8,128)(2,1)S(1)} collective-permute-done((bf16[64,2048]{1,0:T(8,128)(2,1)S(1)}, bf16[64,2048]{1,0:T(8,128)(2,1)S(1)}, u32[]{:S(2)}, u32[]{:S(2)}) %collective-permute-start.22) | collective-permute-done | bytes 262176 | tf_op jit(solution)/shard_map/ppermute | solution.py:47
  156.1 4.4 %collective-permute-start.31 = (bf16[64,2048]{1,0:T(8,128)(2,1)S(1)}, bf16[64,2048]{1,0:T(8,128)(2,1)S(1)}, u32[]{:S(2)}, u32[]{:S(2)}) collective-permute-start(bf16[64,2048]{1,0:T(8,128)(2,1)S(1)} %add_convert_fusion.13), channel_id=1, source_target_pairs={{0,2},{1,3},{6,4},{7,5},{8,10},{9,11},{14,12},{15,13},{16,18},{17,... | collective-permute-start | bytes 786440 | tf_op jit(solution)/shard_map/ppermute | solution.py:47
  167.0 3.2 %collective-permute-done.30 = bf16[64,2048]{1,0:T(8,128)(2,1)S(1)} collective-permute-done((bf16[64,2048]{1,0:T(8,128)(2,1)S(1)}, bf16[64,2048]{1,0:T(8,128)(2,1)S(1)}, u32[]{:S(2)}, u32[]{:S(2)}) %collective-permute-start.30) | collective-permute-done | bytes 262176 | tf_op jit(solution)/shard_map/ppermute | solution.py:47
  170.9 4.1 %collective-permute-done.34 = bf16[64,2048]{1,0:T(8,128)(2,1)S(1)} collective-permute-done((bf16[64,2048]{1,0:T(8,128)(2,1)S(1)}, bf16[64,2048]{1,0:T(8,128)(2,1)S(1)}, u32[]{:S(2)}, u32[]{:S(2)}) %collective-permute-start.34) | collective-permute-done | bytes 262176 | tf_op jit(solution)/shard_map/ppermute | solution.py:47
  177.2 3.0 %collective-permute-done.37.refs_2_ = bf16[32,2048]{1,0:T(8,128)(2,1)S(1)} collective-permute-done((bf16[32,2048]{1,0:T(8,128)(2,1)S(1)}, bf16[32,2048]{1,0:T(8,128)(2,1)S(1)}, u32[]{:S(2)}, u32[]{:S(2)}) %collective-permute-start.37) | collective-permute-done | bytes 131104 | tf_op jit(solution)/shard_map/ppermute | solution.py:500
  (114 shorter events, 27.8 us)
Async XLA Ops:
  2.0 7.8 %collective-permute-start.3 = (bf16[256,128]{1,0:T(8,128)(2,1)}, bf16[256,128]{1,0:T(8,128)(2,1)S(1)}, u32[]{:S(2)}, u32[]{:S(2)}) collective-permute-start(bf16[256,128]{1,0:T(8,128)(2,1)} %last_rows.1), channel_id=1, source_target_pairs={{0,8},{8,16},{16,24},{1,9},{9,17},{17,25},{2,10},{10,18},{18,26},{... | collective-permute-start | bytes 196616 | tf_op jit(solution)/shard_map/ppermute | solution.py:503
  18.7 24.1 %collective-permute-start.4 = (bf16[4,128,2048]{2,1,0:T(8,128)(2,1)}, bf16[4,128,2048]{2,1,0:T(8,128)(2,1)S(1)}, u32[]{:S(2)}, u32[]{:S(2)}) collective-permute-start(bf16[4,128,2048]{2,1,0:T(8,128)(2,1)} %attention.2), channel_id=1, source_target_pairs={{0,1},{1,0},{2,3},{3,2},{4,5},{5,4},{6,7},{7,6},{8,9},{9,8},{10,11... | collective-permute-start | bytes 6291464 | tf_op jit(solution)/shard_map/ppermute | solution.py:52
  18.7 6.3 %collective-permute-start = (bf16[32,2048]{1,0:T(8,128)(2,1)S(1)}, bf16[32,2048]{1,0:T(8,128)(2,1)S(1)}, u32[]{:S(2)}, u32[]{:S(2)}) collective-permute-start(bf16[32,2048]{1,0:T(8,128)(2,1)S(1)} %copy-done.17), channel_id=1, source_target_pairs={{0,8},{8,0},{16,24},{24,16},{1,9},{9,1},{17,25},{25,17},{2,10},{10... | collective-permute-start | bytes 393224 | tf_op jit(solution)/shard_map/ppermute | solution.py:500
  20.3 7.4 %collective-permute-start.1 = (bf16[32,2048]{1,0:T(8,128)(2,1)S(1)}, bf16[32,2048]{1,0:T(8,128)(2,1)S(1)}, u32[]{:S(2)}, u32[]{:S(2)}) collective-permute-start(bf16[32,2048]{1,0:T(8,128)(2,1)S(1)} %copy-done.16), channel_id=1, source_target_pairs={{0,16},{8,24},{16,0},{24,8},{1,17},{9,25},{17,1},{25,9},{2,18},{10... | collective-permute-start | bytes 393224 | tf_op jit(solution)/shard_map/ppermute | solution.py:500
  21.8 7.5 %collective-permute-start.2 = (bf16[32,2048]{1,0:T(8,128)(2,1)S(1)}, bf16[32,2048]{1,0:T(8,128)(2,1)S(1)}, u32[]{:S(2)}, u32[]{:S(2)}) collective-permute-start(bf16[32,2048]{1,0:T(8,128)(2,1)S(1)} %copy-done.15), channel_id=1, source_target_pairs={{0,24},{8,16},{16,8},{24,0},{1,25},{9,17},{17,9},{25,1},{2,26},{10... | collective-permute-start | bytes 393224 | tf_op jit(solution)/shard_map/ppermute | solution.py:500
  29.3 13.5 %collective-permute-start.6 = (bf16[128,2048]{1,0:T(8,128)(2,1)S(1)}, bf16[128,2048]{1,0:T(8,128)(2,1)S(1)}, u32[]{:S(2)}, u32[]{:S(2)}) collective-permute-start(bf16[128,2048]{1,0:T(8,128)(2,1)S(1)} %pack.1.refs_0_), channel_id=1, source_target_pairs={{0,2},{1,3},{2,0},{3,1},{4,6},{5,7},{6,4},{7,5},{8,10},{9,11},{10,... | collective-permute-start | bytes 1572872 | tf_op jit(solution)/shard_map/ppermute | solution.py:47
  31.0 21.8 %collective-permute-start.8 = (bf16[128,2048]{1,0:T(8,128)(2,1)S(1)}, bf16[128,2048]{1,0:T(8,128)(2,1)S(1)}, u32[]{:S(2)}, u32[]{:S(2)}) collective-permute-start(bf16[128,2048]{1,0:T(8,128)(2,1)S(1)} %pack.1.refs_0_), channel_id=1, source_target_pairs={{0,1},{1,0},{2,3},{3,2},{4,5},{5,4},{6,7},{7,6},{8,9},{9,8},{10,11... | collective-permute-start | bytes 1572872 | tf_op jit(solution)/shard_map/ppermute | solution.py:52
  31.0 22.5 %collective-permute-start.12 = (bf16[128,2048]{1,0:T(8,128)(2,1)S(1)}, bf16[128,2048]{1,0:T(8,128)(2,1)S(1)}, u32[]{:S(2)}, u32[]{:S(2)}) collective-permute-start(bf16[128,2048]{1,0:T(8,128)(2,1)S(1)} %pack.1.refs_0_), channel_id=1, source_target_pairs={{2,4},{3,5},{4,2},{5,3},{10,12},{11,13},{12,10},{13,11},{18,20},{1... | collective-permute-start | bytes 1572872 | tf_op jit(solution)/shard_map/ppermute | solution.py:47
  42.8 15.5 %collective-permute-start.7 = (bf16[128,2048]{1,0:T(8,128)(2,1)S(1)}, bf16[128,2048]{1,0:T(8,128)(2,1)S(1)}, u32[]{:S(2)}, u32[]{:S(2)}) collective-permute-start(bf16[128,2048]{1,0:T(8,128)(2,1)S(1)} %collective-permute-done.6.refs_0_), channel_id=1, source_target_pairs={{0,1},{1,0},{2,3},{3,2},{4,5},{5,4},{6,7},{7,6},{8,9},{9,8},{10,11... | collective-permute-start | bytes 1572872 | tf_op jit(solution)/shard_map/ppermute | solution.py:52
  49.3 23.9 %collective-permute-start.5 = (bf16[128,2048]{1,0:T(8,128)(2,1)S(1)}, bf16[128,2048]{1,0:T(8,128)(2,1)S(1)}, u32[]{:S(2)}, u32[]{:S(2)}) collective-permute-start(bf16[128,2048]{1,0:T(8,128)(2,1)S(1)} %get-tuple-element.134), channel_id=1, source_target_pairs={{0,2},{1,3},{6,4},{7,5},{8,10},{9,11},{14,12},{15,13},{16,18},{17,... | collective-permute-start | bytes 1572872 | tf_op jit(solution)/shard_map/ppermute | solution.py:47
  52.8 9.1 %collective-permute-start.10 = (bf16[128,2048]{1,0:T(8,128)(2,1)S(1)}, bf16[128,2048]{1,0:T(8,128)(2,1)S(1)}, u32[]{:S(2)}, u32[]{:S(2)}) collective-permute-start(bf16[128,2048]{1,0:T(8,128)(2,1)S(1)} %collective-permute-done.6.refs_0_), channel_id=1, source_target_pairs={{2,4},{3,5},{4,2},{5,3},{10,12},{11,13},{12,10},{13,11},{18,20},{1... | collective-permute-start | bytes 1572872 | tf_op jit(solution)/shard_map/ppermute | solution.py:47
  53.5 19.7 %collective-permute-start.14 = (bf16[128,2048]{1,0:T(8,128)(2,1)S(1)}, bf16[128,2048]{1,0:T(8,128)(2,1)S(1)}, u32[]{:S(2)}, u32[]{:S(2)}) collective-permute-start(bf16[128,2048]{1,0:T(8,128)(2,1)S(1)} %collective-permute-done.12), channel_id=1, source_target_pairs={{2,0},{3,1},{4,6},{5,7},{10,8},{11,9},{12,14},{13,15},{18,16},{19,... | collective-permute-start | bytes 1572872 | tf_op jit(solution)/shard_map/ppermute | solution.py:47
  61.9 19.5 %collective-permute-start.11 = (bf16[128,2048]{1,0:T(8,128)(2,1)S(1)}, bf16[128,2048]{1,0:T(8,128)(2,1)S(1)}, u32[]{:S(2)}, u32[]{:S(2)}) collective-permute-start(bf16[128,2048]{1,0:T(8,128)(2,1)S(1)} %collective-permute-done.10), channel_id=1, source_target_pairs={{2,0},{3,1},{4,6},{5,7},{10,8},{11,9},{12,14},{13,15},{18,16},{19,... | collective-permute-start | bytes 1572872 | tf_op jit(solution)/shard_map/ppermute | solution.py:47
  63.2 97.4 %collective-permute-start.17 = (bf16[128,2048]{1,0:T(8,128)(2,1)S(1)}, bf16[128,2048]{1,0:T(8,128)(2,1)S(1)}, u32[]{:S(2)}, u32[]{:S(2)}) collective-permute-start(bf16[128,2048]{1,0:T(8,128)(2,1)S(1)} %get-tuple-element.132), channel_id=1, source_target_pairs={{0,2},{1,3},{6,4},{7,5},{8,10},{9,11},{14,12},{15,13},{16,18},{17,... | collective-permute-start | bytes 1572872 | tf_op jit(solution)/shard_map/ppermute | solution.py:47
  71.6 22.2 %collective-permute-start.18 = (bf16[128,2048]{1,0:T(8,128)(2,1)S(1)}, bf16[128,2048]{1,0:T(8,128)(2,1)S(1)}, u32[]{:S(2)}, u32[]{:S(2)}) collective-permute-start(bf16[128,2048]{1,0:T(8,128)(2,1)S(1)} %get-tuple-element.133), channel_id=1, source_target_pairs={{0,2},{1,3},{6,4},{7,5},{8,10},{9,11},{14,12},{15,13},{16,18},{17,... | collective-permute-start | bytes 1572872 | tf_op jit(solution)/shard_map/ppermute | solution.py:47
  73.2 23.4 %collective-permute-start.23 = (bf16[128,2048]{1,0:T(8,128)(2,1)S(1)}, bf16[128,2048]{1,0:T(8,128)(2,1)S(1)}, u32[]{:S(2)}, u32[]{:S(2)}) collective-permute-start(bf16[128,2048]{1,0:T(8,128)(2,1)S(1)} %get-tuple-element.146), channel_id=1, source_target_pairs={{0,1},{1,0},{2,3},{3,2},{4,5},{5,4},{6,7},{7,6},{8,9},{9,8},{10,11... | collective-permute-start | bytes 1572872 | tf_op jit(solution)/shard_map/ppermute | solution.py:52
  73.4 8.3 %collective-permute-start.15 = (bf16[128,2048]{1,0:T(8,128)(2,1)S(1)}, bf16[128,2048]{1,0:T(8,128)(2,1)S(1)}, u32[]{:S(2)}, u32[]{:S(2)}) collective-permute-start(bf16[128,2048]{1,0:T(8,128)(2,1)S(1)} %add_convert_fusion.3.refs_0_), channel_id=1, source_target_pairs={{0,1},{1,0},{2,3},{3,2},{4,5},{5,4},{6,7},{7,6},{8,9},{9,8},{10,11... | collective-permute-start | bytes 1572872 | tf_op jit(solution)/shard_map/ppermute | solution.py:52
  81.7 8.3 %collective-permute-start.9 = (bf16[128,2048]{1,0:T(8,128)(2,1)S(1)}, bf16[128,2048]{1,0:T(8,128)(2,1)S(1)}, u32[]{:S(2)}, u32[]{:S(2)}) collective-permute-start(bf16[128,2048]{1,0:T(8,128)(2,1)S(1)} %add_convert_fusion.5), channel_id=1, source_target_pairs={{4,2},{5,3},{2,4},{3,5},{12,10},{13,11},{10,12},{11,13},{20,18},{2... | collective-permute-start | bytes 1572872 | tf_op jit(solution)/shard_map/ppermute | solution.py:47
  86.0 79.1 %collective-permute-start.29 = (bf16[128,2048]{1,0:T(8,128)(2,1)S(1)}, bf16[128,2048]{1,0:T(8,128)(2,1)S(1)}, u32[]{:S(2)}, u32[]{:S(2)}) collective-permute-start(bf16[128,2048]{1,0:T(8,128)(2,1)S(1)} %get-tuple-element.173), channel_id=1, source_target_pairs={{0,1},{1,0},{2,3},{3,2},{4,5},{5,4},{6,7},{7,6},{8,9},{9,8},{10,11... | collective-permute-start | bytes 1572872 | tf_op jit(solution)/shard_map/ppermute | solution.py:52
  94.0 68.0 %collective-permute-start.16 = (bf16[128,2048]{1,0:T(8,128)(2,1)S(1)}, bf16[128,2048]{1,0:T(8,128)(2,1)S(1)}, u32[]{:S(2)}, u32[]{:S(2)}) collective-permute-start(bf16[128,2048]{1,0:T(8,128)(2,1)S(1)} %add_convert_fusion.2), channel_id=1, source_target_pairs={{2,0},{3,1},{4,6},{5,7},{10,8},{11,9},{12,14},{13,15},{18,16},{19,... | collective-permute-start | bytes 1572872 | tf_op jit(solution)/shard_map/ppermute | solution.py:47
  95.7 67.5 %collective-permute-start.19 = (bf16[128,2048]{1,0:T(8,128)(2,1)S(1)}, bf16[128,2048]{1,0:T(8,128)(2,1)S(1)}, u32[]{:S(2)}, u32[]{:S(2)}) collective-permute-start(bf16[128,2048]{1,0:T(8,128)(2,1)S(1)} %add_convert_fusion.1), channel_id=1, source_target_pairs={{4,2},{5,3},{2,4},{3,5},{12,10},{13,11},{10,12},{11,13},{20,18},{2... | collective-permute-start | bytes 1572872 | tf_op jit(solution)/shard_map/ppermute | solution.py:47
  96.6 15.4 %collective-permute-start.25 = (bf16[64,2048]{1,0:T(8,128)(2,1)S(1)}, bf16[64,2048]{1,0:T(8,128)(2,1)S(1)}, u32[]{:S(2)}, u32[]{:S(2)}) collective-permute-start(bf16[64,2048]{1,0:T(8,128)(2,1)S(1)} %add_convert_fusion.17), channel_id=1, source_target_pairs={{0,2},{1,3},{6,4},{7,5},{8,10},{9,11},{14,12},{15,13},{16,18},{17,... | collective-permute-start | bytes 786440 | tf_op jit(solution)/shard_map/ppermute | solution.py:47
  112.0 9.1 %collective-permute-start.24 = (bf16[64,2048]{1,0:T(8,128)(2,1)S(1)}, bf16[64,2048]{1,0:T(8,128)(2,1)S(1)}, u32[]{:S(2)}, u32[]{:S(2)}) collective-permute-start(bf16[64,2048]{1,0:T(8,128)(2,1)S(1)} %add_convert_fusion.16), channel_id=1, source_target_pairs={{0,2},{1,3},{6,4},{7,5},{8,10},{9,11},{14,12},{15,13},{16,18},{17,... | collective-permute-start | bytes 786440 | tf_op jit(solution)/shard_map/ppermute | solution.py:47
  121.9 15.7 %collective-permute-start.27 = (bf16[64,2048]{1,0:T(8,128)(2,1)S(1)}, bf16[64,2048]{1,0:T(8,128)(2,1)S(1)}, u32[]{:S(2)}, u32[]{:S(2)}) collective-permute-start(bf16[64,2048]{1,0:T(8,128)(2,1)S(1)} %add_convert_fusion.15), channel_id=1, source_target_pairs={{0,2},{1,3},{6,4},{7,5},{8,10},{9,11},{14,12},{15,13},{16,18},{17,... | collective-permute-start | bytes 786440 | tf_op jit(solution)/shard_map/ppermute | solution.py:47
  138.4 17.7 %collective-permute-start.22 = (bf16[64,2048]{1,0:T(8,128)(2,1)S(1)}, bf16[64,2048]{1,0:T(8,128)(2,1)S(1)}, u32[]{:S(2)}, u32[]{:S(2)}) collective-permute-start(bf16[64,2048]{1,0:T(8,128)(2,1)S(1)} %add_convert_fusion.14), channel_id=1, source_target_pairs={{0,2},{1,3},{6,4},{7,5},{8,10},{9,11},{14,12},{15,13},{16,18},{17,... | collective-permute-start | bytes 786440 | tf_op jit(solution)/shard_map/ppermute | solution.py:47
  156.1 10.3 %collective-permute-start.31 = (bf16[64,2048]{1,0:T(8,128)(2,1)S(1)}, bf16[64,2048]{1,0:T(8,128)(2,1)S(1)}, u32[]{:S(2)}, u32[]{:S(2)}) collective-permute-start(bf16[64,2048]{1,0:T(8,128)(2,1)S(1)} %add_convert_fusion.13), channel_id=1, source_target_pairs={{0,2},{1,3},{6,4},{7,5},{8,10},{9,11},{14,12},{15,13},{16,18},{17,... | collective-permute-start | bytes 786440 | tf_op jit(solution)/shard_map/ppermute | solution.py:47
  160.6 10.3 %collective-permute-start.35 = (bf16[64,2048]{1,0:T(8,128)(2,1)S(1)}, bf16[64,2048]{1,0:T(8,128)(2,1)S(1)}, u32[]{:S(2)}, u32[]{:S(2)}) collective-permute-start(bf16[64,2048]{1,0:T(8,128)(2,1)S(1)} %add_convert_fusion.12), channel_id=1, source_target_pairs={{0,2},{1,3},{6,4},{7,5},{8,10},{9,11},{14,12},{15,13},{16,18},{17,... | collective-permute-start | bytes 786440 | tf_op jit(solution)/shard_map/ppermute | solution.py:47
  161.9 8.3 %collective-permute-start.30 = (bf16[64,2048]{1,0:T(8,128)(2,1)S(1)}, bf16[64,2048]{1,0:T(8,128)(2,1)S(1)}, u32[]{:S(2)}, u32[]{:S(2)}) collective-permute-start(bf16[64,2048]{1,0:T(8,128)(2,1)S(1)} %add_convert_fusion.9), channel_id=1, source_target_pairs={{2,0},{3,1},{4,6},{5,7},{10,8},{11,9},{12,14},{13,15},{18,16},{19,... | collective-permute-start | bytes 786440 | tf_op jit(solution)/shard_map/ppermute | solution.py:47
  163.2 7.0 %collective-permute-start.32 = (bf16[64,2048]{1,0:T(8,128)(2,1)S(1)}, bf16[64,2048]{1,0:T(8,128)(2,1)S(1)}, u32[]{:S(2)}, u32[]{:S(2)}) collective-permute-start(bf16[64,2048]{1,0:T(8,128)(2,1)S(1)} %add_convert_fusion.8), channel_id=1, source_target_pairs={{4,2},{5,3},{2,4},{3,5},{12,10},{13,11},{10,12},{11,13},{20,18},{2... | collective-permute-start | bytes 786440 | tf_op jit(solution)/shard_map/ppermute | solution.py:47
  165.1 10.0 %collective-permute-start.34 = (bf16[64,2048]{1,0:T(8,128)(2,1)S(1)}, bf16[64,2048]{1,0:T(8,128)(2,1)S(1)}, u32[]{:S(2)}, u32[]{:S(2)}) collective-permute-start(bf16[64,2048]{1,0:T(8,128)(2,1)S(1)} %add_convert_fusion.7), channel_id=1, source_target_pairs={{2,0},{3,1},{4,6},{5,7},{10,8},{11,9},{12,14},{13,15},{18,16},{19,... | collective-permute-start | bytes 786440 | tf_op jit(solution)/shard_map/ppermute | solution.py:47
  166.4 8.7 %collective-permute-start.36 = (bf16[64,2048]{1,0:T(8,128)(2,1)S(1)}, bf16[64,2048]{1,0:T(8,128)(2,1)S(1)}, u32[]{:S(2)}, u32[]{:S(2)}) collective-permute-start(bf16[64,2048]{1,0:T(8,128)(2,1)S(1)} %add_convert_fusion.6), channel_id=1, source_target_pairs={{4,2},{5,3},{2,4},{3,5},{12,10},{13,11},{10,12},{11,13},{20,18},{2... | collective-permute-start | bytes 786440 | tf_op jit(solution)/shard_map/ppermute | solution.py:47
  170.4 6.8 %collective-permute-start.33 = (bf16[32,2048]{1,0:T(8,128)(2,1)S(1)}, bf16[32,2048]{1,0:T(8,128)(2,1)S(1)}, u32[]{:S(2)}, u32[]{:S(2)}) collective-permute-start(bf16[32,2048]{1,0:T(8,128)(2,1)S(1)} %get-tuple-element.188), channel_id=1, source_target_pairs={{0,8},{8,0},{16,24},{24,16},{1,9},{9,1},{17,25},{25,17},{2,10},{10... | collective-permute-start | bytes 393224 | tf_op jit(solution)/shard_map/ppermute | solution.py:500
  (25 other events, 444.0 us)

commit v3 on v2

--- a/solution.py
+++ b/solution.py
@@ -94,7 +94,8 @@
         self.got = {}
 
     def send(self, values, pairs):
-        out = add_all(self.seq.after(*values))
+        values = self.seq.after(*values)
+        out = add_all(values)
         if len(values) > 1:
             self.seq.did(out)
         return along(out, pairs)
@@ -161,7 +162,14 @@
     )(keys, values)
 
 
-def dispatch_kernel(capacity, block, me_ref, x_ref, gain_ref, ids_ref, share_ref, *out_refs):
+def dispatch_kernel(capacity, block, count, me_ref, x_ref, gain_ref, ids_ref, share_ref, *refs):
+    sources, sems = refs[:count], refs[-1]
+    out_refs, held = refs[count : -1 - count], refs[-1 - count : -1]
+    copies = [
+        pltpu.make_async_copy(a, b, sems.at[i]) for i, (a, b) in enumerate(zip(sources, held))
+    ]
+    for copy in copies:
+        copy.start()
     rows = len(out_refs) * block
     tokens = x_ref.shape[0]
     lanes = 128
@@ -186,13 +194,15 @@
         part = slice(g * block, (g + 1) * block)
         out_ref[:, :lanes] = (out[part, :lanes] + tail[part]).astype(BF)
         out_ref[:, lanes:] = out[part, lanes:].astype(BF)
+    for copy in copies:
+        copy.wait()
 
 
 def in_vmem(count):
     return [pl.BlockSpec(memory_space=pltpu.VMEM)] * count
 
 
-def dispatch(me, x, gain, ids, share, n_groups, capacity, block):
+def dispatch(me, x, gain, ids, share, n_groups, capacity, block, keep):
     gain = gain.reshape(1, -1)
 
     def whole(shape):
@@ -200,15 +210,18 @@
 
     outs = [(block, x.shape[1])] * n_groups
     return pl.pallas_call(
-        functools.partial(dispatch_kernel, capacity, block),
+        functools.partial(dispatch_kernel, capacity, block, len(keep)),
         grid=(1,),
         in_specs=[pl.BlockSpec(memory_space=pltpu.SMEM)]
-        + [whole(v.shape) for v in (x, gain, ids, share)],
-        out_specs=[whole(o) for o in outs],
-        out_shape=[jax.ShapeDtypeStruct(o, BF) for o in outs],
-        compiler_params=pltpu.CompilerParams(vmem_limit_bytes=60 << 20),
+        + [whole(v.shape) for v in (x, gain, ids, share)]
+        + [pl.BlockSpec(memory_space=pltpu.HBM)] * len(keep),
+        out_specs=[whole(o) for o in outs] + in_vmem(len(keep)),
+        out_shape=[jax.ShapeDtypeStruct(o, BF) for o in outs]
+        + [pltpu.VMEM(v.shape, v.dtype) for v in keep],
+        scratch_shapes=[pltpu.SemaphoreType.DMA((len(keep),))],
+        compiler_params=pltpu.CompilerParams(vmem_limit_bytes=61 << 20),
         name="dispatch",
-    )(me, x, gain, ids, share)
+    )(me, x, gain, ids, share, *keep)
 
 
 def pack_kernel(*refs):
@@ -417,23 +430,20 @@
 
 
 def attention_partials(
-    order, base, queries, keys, values, tails, sinks, weight, blocks, plus=None
+    order, base, queries, keys, values, tails, sinks, weight, tables, plus=None
 ):
     width = queries.shape[1]
     narrow = keys.shape[1]
     kv_here = narrow // HD
     per_group = width // narrow
     count = order.shape[0]
-    steps, bases, turn = rotary_tables(width, blocks)
-    many = math.gcd(count, 2)
+    many = count
     operands = (
         queries,
         keys,
         values,
         tails,
-        jnp.asarray(steps),
-        jnp.asarray(bases),
-        jnp.asarray(turn, BF),
+        *tables,
         weight,
     )
 
@@ -442,7 +452,7 @@
 
     out_width = weight.shape[1]
     stack = pl.BlockSpec((many, WINDOW, out_width), lambda i, o, b, s: (i, 0, 0))
-    in_specs = [fixed(x) for x in operands]
+    in_specs = in_vmem(3) + [fixed(tails)] + in_vmem(4)
     if plus is None:
         out_specs, out_shape = stack, jax.ShapeDtypeStruct((count, WINDOW, out_width), BF)
     else:
@@ -464,7 +474,7 @@
             bytes_accessed=2 * weight.size + 2 * count * WINDOW * (weight.shape[1] + 2 * width),
             transcendentals=count * WINDOW * 2 * WINDOW * kv_here * per_group,
         ),
-        compiler_params=pltpu.CompilerParams(vmem_limit_bytes=(60 if plus is None else 28) << 20),
+        compiler_params=pltpu.CompilerParams(vmem_limit_bytes=28 << 20),
         name="attention",
     )(order, base, sinks, *operands)
 
@@ -502,14 +512,19 @@
     tails = seq.did(last_rows(key_rows, value_rows))
     before = lax.ppermute(tails, "ep", [(i, i + 1) for i in range(n_groups - 1)])
     (x,) = seq.after(expert_input)
-    send = dispatch(me, x, norm_gain, ids, route_weight.T, n_groups, capacity, block)
+    tables = rotary_tables(queries.shape[1], n_groups * n_tp)
+    tables = [jnp.asarray(v, d) for v, d in zip(tables, (F32, F32, BF))]
+    keep = (queries, key_rows, value_rows, out_weight, *tables)
+    done = dispatch(me, x, norm_gain, ids, route_weight.T, n_groups, capacity, block, keep)
+    send, (queries, key_rows, value_rows, out_weight, *tables) = done[:n_groups], done[n_groups:]
     seq.did(send[0])
     got = [send[0]] + [around(send[k], k) for k in range(1, n_groups)]
 
     chunk = jnp.stack([slot_chunk(n, z, k) for k in range(n)]) * CORES
 
     def attend(order, plus=None):
-        (q,) = seq.after(queries)
+        q = queries
+        (order,) = seq.after(order)
         return attention_partials(
             order,
             (e * n_tp).reshape(1),
@@ -519,7 +534,7 @@
             before,
             sink_logits,
             out_weight,
-            n_groups * n_tp,
+            tables,
             plus,
         )
 
@@ -565,17 +580,14 @@
     attn = [[v] for v in mine]
     attn_scatter = LineScatter(n, seq)
     for s in range(1, n):
+        attn_scatter.start(s, attn[n - s])
+    for s in range(1, n):
         if s < n - 1:
             gather(s + 1)
+        if s > 1:
+            attn_scatter.step(s, attn)
         prepare(s)
-        if s == 1:
-            for a in range(1, n):
-                attn_scatter.start(a, attn[n - a])
-        elif s < n - 1:
-            attn_scatter.step(s, attn)
         experts([k for k in slots if k not in back])
-    attn_scatter.step(n - 1, attn)
-
     half = n_groups * block // 2
     lines = []
     for h in range(2):

time: 185 us -> 194 us (1.049)
  waiting for transfers between devices: 60.2 us -> 70.1 us
  starting transfers between devices: 83.4 us -> 88.3 us
  Pallas kernels: 32.6 us -> 29.4 us
    ppermute x23, waiting for transfers between devices: 48.8 us -> 57.9 us  [along(): return lax.ppermute(value, 'tp', full)]
    pallas_call x2, Pallas kernels: 13.6 us -> 9.17 us  [attention_partials(): pl.pallas_call(functools.partial(attention_kernel, kv_here, per_group, ma...]
    ppermute x23, starting transfers between devices: 70.6 us -> 74.8 us  [along(): return lax.ppermute(value, 'tp', full)]
  transfers between devices with their start and end apart: 39 -> 39, of which waited for: 15 -> 15; matrix products, arithmetic and copies ran while one was open for 2% -> 2% of each run, Pallas kernels for 12% -> 10%
where the time goes in v3:
time: 194 us; the launch traced here: 193 us
  starting transfers between devices  88.3 us (46%)
  waiting for transfers between devices  70.1 us (36%)
  Pallas kernels  29.4 us (15%)
  other arithmetic  3.22 us (2%)
    ppermute x23, starting transfers between devices, along(): return lax.ppermute(value, 'tp', full)  74.8 us
    ppermute x23, waiting for transfers between devices, along(): return lax.ppermute(value, 'tp', full)  57.9 us
    pallas_call x4, Pallas kernels, expert_rows(): pl.pallas_call(functools.partial(expert_kernel, capacity, block, count),...  14.1 us
    ppermute x6, waiting for transfers between devices, around(): return lax.ppermute(part, 'ep', [(i, i ^ k) for i in range(n_groups)])  10.7 us
    pallas_call x2, Pallas kernels, attention_partials(): pl.pallas_call(functools.partial(attention_kernel, kv_here, per_group, ma...  9.17 us
    ppermute x6, starting transfers between devices, around(): return lax.ppermute(part, 'ep', [(i, i ^ k) for i in range(n_groups)])  7.11 us
    ppermute x1, starting transfers between devices, body(): lax.ppermute(tails, 'ep', [(i, i + 1) for i in range(n_groups - 1)])  4.86 us
  transfers between devices with their start and end apart: 39, of which 15 were waited for; matrix products, arithmetic and copies ran while one was open for 2% of the time, Pallas kernels for 10%

profile of v3, /device:TPU:0, one launch (start us, length us, event | category | flops | bytes accessed | tf_op | source)
XLA Modules:
  0.0 193.0 jit_solution(11293465321517372430)
XLA Ops:
  2.0 4.9 %collective-permute-start.3 = (bf16[256,128]{1,0:T(8,128)(2,1)}, bf16[256,128]{1,0:T(8,128)(2,1)S(1)}, u32[]{:S(2)}, u32[]{:S(2)}) collective-permute-start(bf16[256,128]{1,0:T(8,128)(2,1)} %last_rows.1), channel_id=1, source_target_pairs={{0,8},{8,16},{16,24},{1,9},{9,17},{17,25},{2,10},{10,18},{18,26},{... | collective-permute-start | bytes 196616 | tf_op jit(solution)/shard_map/ppermute | solution.py:513
  7.0 3.5 %dispatch.1 = (bf16[32,2048]{1,0:T(8,128)(2,1)}, bf16[32,2048]{1,0:T(8,128)(2,1)}, bf16[32,2048]{1,0:T(8,128)(2,1)}, bf16[32,2048]{1,0:T(8,128)(2,1)}, bf16[1024...) custom-call(s32[1]{0:T(128)} %bitcast.4.me_ref, ...), custom_call_target="tpu_custom_call" | custom-call | tf_op jit(solution)/shard_map/dispatch/pallas_call | solution.py:212
  11.3 4.5 %attention.2 = bf16[4,128,2048]{2,1,0:T(8,128)(2,1)S(1)} custom-call(s32[4]{0:T(128)S(1)} %get-tuple-element.105.order_ref, s32[1]{0:T(128)} %bitcast.8.base_ref, f32[4]{0:T(128)S(1)} %copy-done.5, bf16[1024,256]{1,0:T(8,128)(2,1)S(1)} %get-tuple-element.106.q_ref, bf16[1024,128]{1,0:T(8,128)(2,1)S(1)} %get-tuple-element.107.k_ref, ...), custom_call_target="tpu_custom_call" | custom-call | flops 5368709120 | bytes 3670016 | tf_op jit(solution)/shard_map/attention/pallas_call | solution.py:463
  15.9 1.6 collective-permute-start
  19.5 2.7 %collective-permute-done.refs_1_ = bf16[32,2048]{1,0:T(8,128)(2,1)S(1)} collective-permute-done((bf16[32,2048]{1,0:T(8,128)(2,1)S(1)}, bf16[32,2048]{1,0:T(8,128)(2,1)S(1)}, u32[]{:S(2)}, u32[]{:S(2)}) %collective-permute-start) | collective-permute-done | bytes 131104 | tf_op jit(solution)/shard_map/ppermute | solution.py:510
  22.2 2.0 %collective-permute-done.1.refs_2_ = bf16[32,2048]{1,0:T(8,128)(2,1)S(1)} collective-permute-done((bf16[32,2048]{1,0:T(8,128)(2,1)S(1)}, bf16[32,2048]{1,0:T(8,128)(2,1)S(1)}, u32[]{:S(2)}, u32[]{:S(2)}) %collective-permute-start.1) | collective-permute-done | bytes 131104 | tf_op jit(solution)/shard_map/ppermute | solution.py:510
  24.2 1.7 collective-permute-done.2.refs_3_
  25.9 1.6 collective-permute-start.6
  28.3 11.0 %collective-permute-done.6.refs_0_ = bf16[128,2048]{1,0:T(8,128)(2,1)S(1)} collective-permute-done((bf16[128,2048]{1,0:T(8,128)(2,1)S(1)}, bf16[128,2048]{1,0:T(8,128)(2,1)S(1)}, u32[]{:S(2)}, u32[]{:S(2)}) %collective-permute-start.6) | collective-permute-done | bytes 524320 | tf_op jit(solution)/shard_map/ppermute | solution.py:47
  39.3 4.6 %attention.3 = (bf16[128,2048]{1,0:T(8,128)(2,1)S(1)}, bf16[128,2048]{1,0:T(8,128)(2,1)S(1)}, bf16[128,2048]{1,0:T(8,128)(2,1)S(1)}, bf16[128,2048]{1,0:T(8,128)(2,1)S(1)}) custom-call(s32[4]{0:T(128)S(1)} %broadcast_add_fusion.order_ref, s32[1]{0:T(128)} %bitcast.8.base_ref, f32[4]{0:T(128)S(1)} %copy-done.5, ...), custom_call_target="tpu_custom_call" | custom-call | flops 5368709120 | bytes 3670016 | tf_op jit(solution)/shard_map/attention/pallas_call | solution.py:463
  46.0 3.6 %experts.4 = (bf16[128,2048]{1,0:T(8,128)(2,1)S(1)}, bf16[128,2048]{1,0:T(8,128)(2,1)S(1)}) custom-call(bf16[128,2048]{1,0:T(8,128)(2,1)S(1)} %pack.1.refs_0_, bf16[128,2048]{1,0:T(8,128)(2,1)S(1)} %collective-permute-done.8.refs_1_, bf16[2,2048,512]{2,1,0:T(8,128)(2,1)S(1)} %copy-done, bf16[2,2048,512]{2,1,0:T(8,128)(2,1)S(1)} %copy-done.1, ...), custom_call_target="tpu_custom_call" | custom-call | flops 3221225472 | bytes 2097152 | tf_op jit(solution)/shard_map/experts/pallas_call | solution.py:305
  49.6 6.3 %collective-permute-start.16 = (bf16[128,2048]{1,0:T(8,128)(2,1)S(1)}, bf16[128,2048]{1,0:T(8,128)(2,1)S(1)}, u32[]{:S(2)}, u32[]{:S(2)}) collective-permute-start(bf16[128,2048]{1,0:T(8,128)(2,1)S(1)} %get-tuple-element.143), channel_id=1, source_target_pairs={{0,2},{1,3},{6,4},{7,5},{8,10},{9,11},{14,12},{15,13},{16,18},{17,... | collective-permute-start | bytes 1572872 | tf_op jit(solution)/shard_map/ppermute | solution.py:47
  55.9 1.5 collective-permute-start.5
  57.4 3.5 %experts.5 = (bf16[128,2048]{1,0:T(8,128)(2,1)S(1)}, bf16[128,2048]{1,0:T(8,128)(2,1)S(1)}) custom-call(bf16[128,2048]{1,0:T(8,128)(2,1)S(1)} %collective-permute-done.6.refs_0_, bf16[128,2048]{1,0:T(8,128)(2,1)S(1)} %collective-permute-done.7.refs_1_, bf16[2,2048,512]{2,1,0:T(8,128)(2,1)S(1)} %copy-done, bf16[2,2048,512]{2,1,0:T(8,128)(2,1)S(1)} %copy-done.1, ...), custom_call_target="tpu_custom_call" | custom-call | flops 3221225472 | bytes 2097152 | tf_op jit(solution)/shard_map/experts/pallas_call | solution.py:305
  62.8 15.8 %collective-permute-done.5 = bf16[128,2048]{1,0:T(8,128)(2,1)S(1)} collective-permute-done((bf16[128,2048]{1,0:T(8,128)(2,1)S(1)}, bf16[128,2048]{1,0:T(8,128)(2,1)S(1)}, u32[]{:S(2)}, u32[]{:S(2)}) %collective-permute-start.5) | collective-permute-done | bytes 524320 | tf_op jit(solution)/shard_map/ppermute | solution.py:47
  79.7 3.5 %experts.6 = (bf16[128,2048]{1,0:T(8,128)(2,1)S(1)}, bf16[128,2048]{1,0:T(8,128)(2,1)S(1)}) custom-call(bf16[128,2048]{1,0:T(8,128)(2,1)S(1)} %add_convert_fusion.4.refs_0_, bf16[128,2048]{1,0:T(8,128)(2,1)S(1)} %collective-permute-done.13.refs_1_, bf16[2,2048,512]{2,1,0:T(8,128)(2,1)S(1)} %copy-done, bf16[2,2048,512]{2,1,0:T(8,128)(2,1)S(1)} %copy-done.1, ...), custom_call_target="tpu_custom_call" | custom-call | flops 3221225472 | bytes 2097152 | tf_op jit(solution)/shard_map/experts/pallas_call | solution.py:305
  83.5 3.5 %experts.7 = (bf16[128,2048]{1,0:T(8,128)(2,1)S(1)}, bf16[128,2048]{1,0:T(8,128)(2,1)S(1)}) custom-call(bf16[128,2048]{1,0:T(8,128)(2,1)S(1)} %add_convert_fusion.1.refs_0_, bf16[128,2048]{1,0:T(8,128)(2,1)S(1)} %collective-permute-done.19.refs_1_, bf16[2,2048,512]{2,1,0:T(8,128)(2,1)S(1)} %copy-done, bf16[2,2048,512]{2,1,0:T(8,128)(2,1)S(1)} %copy-done.1, ...), custom_call_target="tpu_custom_call" | custom-call | flops 3221225472 | bytes 2097152 | tf_op jit(solution)/shard_map/experts/pallas_call | solution.py:305
  87.7 14.9 %collective-permute-start.15 = (bf16[128,2048]{1,0:T(8,128)(2,1)S(1)}, bf16[128,2048]{1,0:T(8,128)(2,1)S(1)}, u32[]{:S(2)}, u32[]{:S(2)}) collective-permute-start(bf16[128,2048]{1,0:T(8,128)(2,1)S(1)} %get-tuple-element.142), channel_id=1, source_target_pairs={{0,2},{1,3},{6,4},{7,5},{8,10},{9,11},{14,12},{15,13},{16,18},{17,... | collective-permute-start | bytes 1572872 | tf_op jit(solution)/shard_map/ppermute | solution.py:47
  107.0 4.6 %collective-permute-start.25 = (bf16[64,2048]{1,0:T(8,128)(2,1)S(1)}, bf16[64,2048]{1,0:T(8,128)(2,1)S(1)}, u32[]{:S(2)}, u32[]{:S(2)}) collective-permute-start(bf16[64,2048]{1,0:T(8,128)(2,1)S(1)} %add_convert_fusion.17), channel_id=1, source_target_pairs={{0,2},{1,3},{6,4},{7,5},{8,10},{9,11},{14,12},{15,13},{16,18},{17,... | collective-permute-start | bytes 786440 | tf_op jit(solution)/shard_map/ppermute | solution.py:47
  111.7 7.9 %collective-permute-done.25 = bf16[64,2048]{1,0:T(8,128)(2,1)S(1)} collective-permute-done((bf16[64,2048]{1,0:T(8,128)(2,1)S(1)}, bf16[64,2048]{1,0:T(8,128)(2,1)S(1)}, u32[]{:S(2)}, u32[]{:S(2)}) %collective-permute-start.25) | collective-permute-done | bytes 262176 | tf_op jit(solution)/shard_map/ppermute | solution.py:47
  119.7 4.4 %collective-permute-start.24 = (bf16[64,2048]{1,0:T(8,128)(2,1)S(1)}, bf16[64,2048]{1,0:T(8,128)(2,1)S(1)}, u32[]{:S(2)}, u32[]{:S(2)}) collective-permute-start(bf16[64,2048]{1,0:T(8,128)(2,1)S(1)} %add_convert_fusion.16), channel_id=1, source_target_pairs={{0,2},{1,3},{6,4},{7,5},{8,10},{9,11},{14,12},{15,13},{16,18},{17,... | collective-permute-start | bytes 786440 | tf_op jit(solution)/shard_map/ppermute | solution.py:47
  124.2 4.8 %collective-permute-done.24 = bf16[64,2048]{1,0:T(8,128)(2,1)S(1)} collective-permute-done((bf16[64,2048]{1,0:T(8,128)(2,1)S(1)}, bf16[64,2048]{1,0:T(8,128)(2,1)S(1)}, u32[]{:S(2)}, u32[]{:S(2)}) %collective-permute-start.24) | collective-permute-done | bytes 262176 | tf_op jit(solution)/shard_map/ppermute | solution.py:47
  129.8 12.1 %collective-permute-start.27 = (bf16[64,2048]{1,0:T(8,128)(2,1)S(1)}, bf16[64,2048]{1,0:T(8,128)(2,1)S(1)}, u32[]{:S(2)}, u32[]{:S(2)}) collective-permute-start(bf16[64,2048]{1,0:T(8,128)(2,1)S(1)} %add_convert_fusion.15), channel_id=1, source_target_pairs={{0,2},{1,3},{6,4},{7,5},{8,10},{9,11},{14,12},{15,13},{16,18},{17,... | collective-permute-start | bytes 786440 | tf_op jit(solution)/shard_map/ppermute | solution.py:47
  141.9 3.8 %collective-permute-done.27 = bf16[64,2048]{1,0:T(8,128)(2,1)S(1)} collective-permute-done((bf16[64,2048]{1,0:T(8,128)(2,1)S(1)}, bf16[64,2048]{1,0:T(8,128)(2,1)S(1)}, u32[]{:S(2)}, u32[]{:S(2)}) %collective-permute-start.27) | collective-permute-done | bytes 262176 | tf_op jit(solution)/shard_map/ppermute | solution.py:47
  146.5 11.8 %collective-permute-start.22 = (bf16[64,2048]{1,0:T(8,128)(2,1)S(1)}, bf16[64,2048]{1,0:T(8,128)(2,1)S(1)}, u32[]{:S(2)}, u32[]{:S(2)}) collective-permute-start(bf16[64,2048]{1,0:T(8,128)(2,1)S(1)} %add_convert_fusion.14), channel_id=1, source_target_pairs={{0,2},{1,3},{6,4},{7,5},{8,10},{9,11},{14,12},{15,13},{16,18},{17,... | collective-permute-start | bytes 786440 | tf_op jit(solution)/shard_map/ppermute | solution.py:47
  158.4 5.2 %collective-permute-done.22 = bf16[64,2048]{1,0:T(8,128)(2,1)S(1)} collective-permute-done((bf16[64,2048]{1,0:T(8,128)(2,1)S(1)}, bf16[64,2048]{1,0:T(8,128)(2,1)S(1)}, u32[]{:S(2)}, u32[]{:S(2)}) %collective-permute-start.22) | collective-permute-done | bytes 262176 | tf_op jit(solution)/shard_map/ppermute | solution.py:47
  163.7 4.4 %collective-permute-start.31 = (bf16[64,2048]{1,0:T(8,128)(2,1)S(1)}, bf16[64,2048]{1,0:T(8,128)(2,1)S(1)}, u32[]{:S(2)}, u32[]{:S(2)}) collective-permute-start(bf16[64,2048]{1,0:T(8,128)(2,1)S(1)} %add_convert_fusion.13), channel_id=1, source_target_pairs={{0,2},{1,3},{6,4},{7,5},{8,10},{9,11},{14,12},{15,13},{16,18},{17,... | collective-permute-start | bytes 786440 | tf_op jit(solution)/shard_map/ppermute | solution.py:47
  174.6 3.8 %collective-permute-done.30 = bf16[64,2048]{1,0:T(8,128)(2,1)S(1)} collective-permute-done((bf16[64,2048]{1,0:T(8,128)(2,1)S(1)}, bf16[64,2048]{1,0:T(8,128)(2,1)S(1)}, u32[]{:S(2)}, u32[]{:S(2)}) %collective-permute-start.30) | collective-permute-done | bytes 262176 | tf_op jit(solution)/shard_map/ppermute | solution.py:47
  178.6 5.2 %collective-permute-done.34 = bf16[64,2048]{1,0:T(8,128)(2,1)S(1)} collective-permute-done((bf16[64,2048]{1,0:T(8,128)(2,1)S(1)}, bf16[64,2048]{1,0:T(8,128)(2,1)S(1)}, u32[]{:S(2)}, u32[]{:S(2)}) %collective-permute-start.34) | collective-permute-done | bytes 262176 | tf_op jit(solution)/shard_map/ppermute | solution.py:47
  184.3 1.6 collective-permute-start.38
  185.9 1.6 collective-permute-start.33
  187.5 2.9 %collective-permute-done.37.refs_2_ = bf16[32,2048]{1,0:T(8,128)(2,1)S(1)} collective-permute-done((bf16[32,2048]{1,0:T(8,128)(2,1)S(1)}, bf16[32,2048]{1,0:T(8,128)(2,1)S(1)}, u32[]{:S(2)}, u32[]{:S(2)}) %collective-permute-start.37) | collective-permute-done | bytes 131104 | tf_op jit(solution)/shard_map/ppermute | solution.py:510
  (96 shorter events, 26.7 us)
Async XLA Ops:
  2.0 8.6 %collective-permute-start.3 = (bf16[256,128]{1,0:T(8,128)(2,1)}, bf16[256,128]{1,0:T(8,128)(2,1)S(1)}, u32[]{:S(2)}, u32[]{:S(2)}) collective-permute-start(bf16[256,128]{1,0:T(8,128)(2,1)} %last_rows.1), channel_id=1, source_target_pairs={{0,8},{8,16},{16,24},{1,9},{9,17},{17,25},{2,10},{10,18},{18,26},{... | collective-permute-start | bytes 196616 | tf_op jit(solution)/shard_map/ppermute | solution.py:513
  15.8 23.5 %collective-permute-start.4 = (bf16[4,128,2048]{2,1,0:T(8,128)(2,1)S(1)}, bf16[4,128,2048]{2,1,0:T(8,128)(2,1)S(1)}, u32[]{:S(2)}, u32[]{:S(2)}) collective-permute-start(bf16[4,128,2048]{2,1,0:T(8,128)(2,1)S(1)} %attention.2), channel_id=1, source_target_pairs={{0,1},{1,0},{2,3},{3,2},{4,5},{5,4},{6,7},{7,6},{8,9},{9,8},{10,11... | collective-permute-start | bytes 6291464 | tf_op jit(solution)/shard_map/ppermute | solution.py:52
  15.9 6.3 %collective-permute-start = (bf16[32,2048]{1,0:T(8,128)(2,1)S(1)}, bf16[32,2048]{1,0:T(8,128)(2,1)S(1)}, u32[]{:S(2)}, u32[]{:S(2)}) collective-permute-start(bf16[32,2048]{1,0:T(8,128)(2,1)S(1)} %copy-done.8), channel_id=1, source_target_pairs={{0,8},{8,0},{16,24},{24,16},{1,9},{9,1},{17,25},{25,17},{2,10},{10... | collective-permute-start | bytes 393224 | tf_op jit(solution)/shard_map/ppermute | solution.py:510
  17.5 6.7 %collective-permute-start.1 = (bf16[32,2048]{1,0:T(8,128)(2,1)S(1)}, bf16[32,2048]{1,0:T(8,128)(2,1)S(1)}, u32[]{:S(2)}, u32[]{:S(2)}) collective-permute-start(bf16[32,2048]{1,0:T(8,128)(2,1)S(1)} %copy-done.7), channel_id=1, source_target_pairs={{0,16},{8,24},{16,0},{24,8},{1,17},{9,25},{17,1},{25,9},{2,18},{10... | collective-permute-start | bytes 393224 | tf_op jit(solution)/shard_map/ppermute | solution.py:510
  18.3 7.6 %collective-permute-start.2 = (bf16[32,2048]{1,0:T(8,128)(2,1)S(1)}, bf16[32,2048]{1,0:T(8,128)(2,1)S(1)}, u32[]{:S(2)}, u32[]{:S(2)}) collective-permute-start(bf16[32,2048]{1,0:T(8,128)(2,1)S(1)} %copy-done.6), channel_id=1, source_target_pairs={{0,24},{8,16},{16,8},{24,0},{1,25},{9,17},{17,9},{25,1},{2,26},{10... | collective-permute-start | bytes 393224 | tf_op jit(solution)/shard_map/ppermute | solution.py:510
  25.9 13.4 %collective-permute-start.6 = (bf16[128,2048]{1,0:T(8,128)(2,1)S(1)}, bf16[128,2048]{1,0:T(8,128)(2,1)S(1)}, u32[]{:S(2)}, u32[]{:S(2)}) collective-permute-start(bf16[128,2048]{1,0:T(8,128)(2,1)S(1)} %pack.1.refs_0_), channel_id=1, source_target_pairs={{0,2},{1,3},{2,0},{3,1},{4,6},{5,7},{6,4},{7,5},{8,10},{9,11},{10,... | collective-permute-start | bytes 1572872 | tf_op jit(solution)/shard_map/ppermute | solution.py:47
  27.5 17.1 %collective-permute-start.8 = (bf16[128,2048]{1,0:T(8,128)(2,1)S(1)}, bf16[128,2048]{1,0:T(8,128)(2,1)S(1)}, u32[]{:S(2)}, u32[]{:S(2)}) collective-permute-start(bf16[128,2048]{1,0:T(8,128)(2,1)S(1)} %pack.1.refs_0_), channel_id=1, source_target_pairs={{0,1},{1,0},{2,3},{3,2},{4,5},{5,4},{6,7},{7,6},{8,9},{9,8},{10,11... | collective-permute-start | bytes 1572872 | tf_op jit(solution)/shard_map/ppermute | solution.py:52
  27.5 17.1 %collective-permute-start.10 = (bf16[128,2048]{1,0:T(8,128)(2,1)S(1)}, bf16[128,2048]{1,0:T(8,128)(2,1)S(1)}, u32[]{:S(2)}, u32[]{:S(2)}) collective-permute-start(bf16[128,2048]{1,0:T(8,128)(2,1)S(1)} %pack.1.refs_0_), channel_id=1, source_target_pairs={{2,4},{3,5},{4,2},{5,3},{10,12},{11,13},{12,10},{13,11},{18,20},{1... | collective-permute-start | bytes 1572872 | tf_op jit(solution)/shard_map/ppermute | solution.py:47
  39.3 10.3 %collective-permute-start.7 = (bf16[128,2048]{1,0:T(8,128)(2,1)S(1)}, bf16[128,2048]{1,0:T(8,128)(2,1)S(1)}, u32[]{:S(2)}, u32[]{:S(2)}) collective-permute-start(bf16[128,2048]{1,0:T(8,128)(2,1)S(1)} %collective-permute-done.6.refs_0_), channel_id=1, source_target_pairs={{0,1},{1,0},{2,3},{3,2},{4,5},{5,4},{6,7},{7,6},{8,9},{9,8},{10,11... | collective-permute-start | bytes 1572872 | tf_op jit(solution)/shard_map/ppermute | solution.py:52
  43.9 17.0 %collective-permute-start.12 = (bf16[128,2048]{1,0:T(8,128)(2,1)S(1)}, bf16[128,2048]{1,0:T(8,128)(2,1)S(1)}, u32[]{:S(2)}, u32[]{:S(2)}) collective-permute-start(bf16[128,2048]{1,0:T(8,128)(2,1)S(1)} %collective-permute-done.6.refs_0_), channel_id=1, source_target_pairs={{2,4},{3,5},{4,2},{5,3},{10,12},{11,13},{12,10},{13,11},{18,20},{1... | collective-permute-start | bytes 1572872 | tf_op jit(solution)/shard_map/ppermute | solution.py:47
  44.7 17.9 %collective-permute-start.11 = (bf16[128,2048]{1,0:T(8,128)(2,1)S(1)}, bf16[128,2048]{1,0:T(8,128)(2,1)S(1)}, u32[]{:S(2)}, u32[]{:S(2)}) collective-permute-start(bf16[128,2048]{1,0:T(8,128)(2,1)S(1)} %collective-permute-done.10), channel_id=1, source_target_pairs={{2,0},{3,1},{4,6},{5,7},{10,8},{11,9},{12,14},{13,15},{18,16},{19,... | collective-permute-start | bytes 1572872 | tf_op jit(solution)/shard_map/ppermute | solution.py:47
  49.6 33.8 %collective-permute-start.16 = (bf16[128,2048]{1,0:T(8,128)(2,1)S(1)}, bf16[128,2048]{1,0:T(8,128)(2,1)S(1)}, u32[]{:S(2)}, u32[]{:S(2)}) collective-permute-start(bf16[128,2048]{1,0:T(8,128)(2,1)S(1)} %get-tuple-element.143), channel_id=1, source_target_pairs={{0,2},{1,3},{6,4},{7,5},{8,10},{9,11},{14,12},{15,13},{16,18},{17,... | collective-permute-start | bytes 1572872 | tf_op jit(solution)/shard_map/ppermute | solution.py:47
  55.9 22.8 %collective-permute-start.5 = (bf16[128,2048]{1,0:T(8,128)(2,1)S(1)}, bf16[128,2048]{1,0:T(8,128)(2,1)S(1)}, u32[]{:S(2)}, u32[]{:S(2)}) collective-permute-start(bf16[128,2048]{1,0:T(8,128)(2,1)S(1)} %get-tuple-element.144), channel_id=1, source_target_pairs={{0,2},{1,3},{6,4},{7,5},{8,10},{9,11},{14,12},{15,13},{16,18},{17,... | collective-permute-start | bytes 1572872 | tf_op jit(solution)/shard_map/ppermute | solution.py:47
  60.9 18.5 %collective-permute-start.18 = (bf16[128,2048]{1,0:T(8,128)(2,1)S(1)}, bf16[128,2048]{1,0:T(8,128)(2,1)S(1)}, u32[]{:S(2)}, u32[]{:S(2)}) collective-permute-start(bf16[128,2048]{1,0:T(8,128)(2,1)S(1)} %collective-permute-done.12), channel_id=1, source_target_pairs={{2,0},{3,1},{4,6},{5,7},{10,8},{11,9},{12,14},{13,15},{18,16},{19,... | collective-permute-start | bytes 1572872 | tf_op jit(solution)/shard_map/ppermute | solution.py:47
  62.7 17.0 %collective-permute-start.13 = (bf16[128,2048]{1,0:T(8,128)(2,1)S(1)}, bf16[128,2048]{1,0:T(8,128)(2,1)S(1)}, u32[]{:S(2)}, u32[]{:S(2)}) collective-permute-start(bf16[128,2048]{1,0:T(8,128)(2,1)S(1)} %add_convert_fusion.4.refs_0_), channel_id=1, source_target_pairs={{0,1},{1,0},{2,3},{3,2},{4,5},{5,4},{6,7},{7,6},{8,9},{9,8},{10,11... | collective-permute-start | bytes 1572872 | tf_op jit(solution)/shard_map/ppermute | solution.py:52
  87.1 16.4 %collective-permute-start.20 = (bf16[128,2048]{1,0:T(8,128)(2,1)S(1)}, bf16[128,2048]{1,0:T(8,128)(2,1)S(1)}, u32[]{:S(2)}, u32[]{:S(2)}) collective-permute-start(bf16[128,2048]{1,0:T(8,128)(2,1)S(1)} %get-tuple-element.150), channel_id=1, source_target_pairs={{0,1},{1,0},{2,3},{3,2},{4,5},{5,4},{6,7},{7,6},{8,9},{9,8},{10,11... | collective-permute-start | bytes 1572872 | tf_op jit(solution)/shard_map/ppermute | solution.py:52
  87.6 19.4 %collective-permute-start.23 = (bf16[128,2048]{1,0:T(8,128)(2,1)S(1)}, bf16[128,2048]{1,0:T(8,128)(2,1)S(1)}, u32[]{:S(2)}, u32[]{:S(2)}) collective-permute-start(bf16[128,2048]{1,0:T(8,128)(2,1)S(1)} %get-tuple-element.160), channel_id=1, source_target_pairs={{0,1},{1,0},{2,3},{3,2},{4,5},{5,4},{6,7},{7,6},{8,9},{9,8},{10,11... | collective-permute-start | bytes 1572872 | tf_op jit(solution)/shard_map/ppermute | solution.py:52
  87.7 80.5 %collective-permute-start.15 = (bf16[128,2048]{1,0:T(8,128)(2,1)S(1)}, bf16[128,2048]{1,0:T(8,128)(2,1)S(1)}, u32[]{:S(2)}, u32[]{:S(2)}) collective-permute-start(bf16[128,2048]{1,0:T(8,128)(2,1)S(1)} %get-tuple-element.142), channel_id=1, source_target_pairs={{0,2},{1,3},{6,4},{7,5},{8,10},{9,11},{14,12},{15,13},{16,18},{17,... | collective-permute-start | bytes 1572872 | tf_op jit(solution)/shard_map/ppermute | solution.py:47
  102.7 70.0 %collective-permute-start.29 = (bf16[128,2048]{1,0:T(8,128)(2,1)S(1)}, bf16[128,2048]{1,0:T(8,128)(2,1)S(1)}, u32[]{:S(2)}, u32[]{:S(2)}) collective-permute-start(bf16[128,2048]{1,0:T(8,128)(2,1)S(1)} %get-tuple-element.187), channel_id=1, source_target_pairs={{0,1},{1,0},{2,3},{3,2},{4,5},{5,4},{6,7},{7,6},{8,9},{9,8},{10,11... | collective-permute-start | bytes 1572872 | tf_op jit(solution)/shard_map/ppermute | solution.py:52
  102.7 66.7 %collective-permute-start.17 = (bf16[128,2048]{1,0:T(8,128)(2,1)S(1)}, bf16[128,2048]{1,0:T(8,128)(2,1)S(1)}, u32[]{:S(2)}, u32[]{:S(2)}) collective-permute-start(bf16[128,2048]{1,0:T(8,128)(2,1)S(1)} %add_convert_fusion.2), channel_id=1, source_target_pairs={{4,2},{5,3},{2,4},{3,5},{12,10},{13,11},{10,12},{11,13},{20,18},{2... | collective-permute-start | bytes 1572872 | tf_op jit(solution)/shard_map/ppermute | solution.py:47
  105.5 64.6 %collective-permute-start.14 = (bf16[128,2048]{1,0:T(8,128)(2,1)S(1)}, bf16[128,2048]{1,0:T(8,128)(2,1)S(1)}, u32[]{:S(2)}, u32[]{:S(2)}) collective-permute-start(bf16[128,2048]{1,0:T(8,128)(2,1)S(1)} %add_convert_fusion.3), channel_id=1, source_target_pairs={{2,0},{3,1},{4,6},{5,7},{10,8},{11,9},{12,14},{13,15},{18,16},{19,... | collective-permute-start | bytes 1572872 | tf_op jit(solution)/shard_map/ppermute | solution.py:47
  107.0 12.7 %collective-permute-start.25 = (bf16[64,2048]{1,0:T(8,128)(2,1)S(1)}, bf16[64,2048]{1,0:T(8,128)(2,1)S(1)}, u32[]{:S(2)}, u32[]{:S(2)}) collective-permute-start(bf16[64,2048]{1,0:T(8,128)(2,1)S(1)} %add_convert_fusion.17), channel_id=1, source_target_pairs={{0,2},{1,3},{6,4},{7,5},{8,10},{9,11},{14,12},{15,13},{16,18},{17,... | collective-permute-start | bytes 786440 | tf_op jit(solution)/shard_map/ppermute | solution.py:47
  119.7 9.3 %collective-permute-start.24 = (bf16[64,2048]{1,0:T(8,128)(2,1)S(1)}, bf16[64,2048]{1,0:T(8,128)(2,1)S(1)}, u32[]{:S(2)}, u32[]{:S(2)}) collective-permute-start(bf16[64,2048]{1,0:T(8,128)(2,1)S(1)} %add_convert_fusion.16), channel_id=1, source_target_pairs={{0,2},{1,3},{6,4},{7,5},{8,10},{9,11},{14,12},{15,13},{16,18},{17,... | collective-permute-start | bytes 786440 | tf_op jit(solution)/shard_map/ppermute | solution.py:47
  129.8 15.9 %collective-permute-start.27 = (bf16[64,2048]{1,0:T(8,128)(2,1)S(1)}, bf16[64,2048]{1,0:T(8,128)(2,1)S(1)}, u32[]{:S(2)}, u32[]{:S(2)}) collective-permute-start(bf16[64,2048]{1,0:T(8,128)(2,1)S(1)} %add_convert_fusion.15), channel_id=1, source_target_pairs={{0,2},{1,3},{6,4},{7,5},{8,10},{9,11},{14,12},{15,13},{16,18},{17,... | collective-permute-start | bytes 786440 | tf_op jit(solution)/shard_map/ppermute | solution.py:47
  146.5 17.2 %collective-permute-start.22 = (bf16[64,2048]{1,0:T(8,128)(2,1)S(1)}, bf16[64,2048]{1,0:T(8,128)(2,1)S(1)}, u32[]{:S(2)}, u32[]{:S(2)}) collective-permute-start(bf16[64,2048]{1,0:T(8,128)(2,1)S(1)} %add_convert_fusion.14), channel_id=1, source_target_pairs={{0,2},{1,3},{6,4},{7,5},{8,10},{9,11},{14,12},{15,13},{16,18},{17,... | collective-permute-start | bytes 786440 | tf_op jit(solution)/shard_map/ppermute | solution.py:47
  163.7 9.6 %collective-permute-start.31 = (bf16[64,2048]{1,0:T(8,128)(2,1)S(1)}, bf16[64,2048]{1,0:T(8,128)(2,1)S(1)}, u32[]{:S(2)}, u32[]{:S(2)}) collective-permute-start(bf16[64,2048]{1,0:T(8,128)(2,1)S(1)} %add_convert_fusion.13), channel_id=1, source_target_pairs={{0,2},{1,3},{6,4},{7,5},{8,10},{9,11},{14,12},{15,13},{16,18},{17,... | collective-permute-start | bytes 786440 | tf_op jit(solution)/shard_map/ppermute | solution.py:47
  168.2 10.5 %collective-permute-start.35 = (bf16[64,2048]{1,0:T(8,128)(2,1)S(1)}, bf16[64,2048]{1,0:T(8,128)(2,1)S(1)}, u32[]{:S(2)}, u32[]{:S(2)}) collective-permute-start(bf16[64,2048]{1,0:T(8,128)(2,1)S(1)} %add_convert_fusion.12), channel_id=1, source_target_pairs={{0,2},{1,3},{6,4},{7,5},{8,10},{9,11},{14,12},{15,13},{16,18},{17,... | collective-permute-start | bytes 786440 | tf_op jit(solution)/shard_map/ppermute | solution.py:47
  170.2 8.3 %collective-permute-start.30 = (bf16[64,2048]{1,0:T(8,128)(2,1)S(1)}, bf16[64,2048]{1,0:T(8,128)(2,1)S(1)}, u32[]{:S(2)}, u32[]{:S(2)}) collective-permute-start(bf16[64,2048]{1,0:T(8,128)(2,1)S(1)} %add_convert_fusion.9), channel_id=1, source_target_pairs={{2,0},{3,1},{4,6},{5,7},{10,8},{11,9},{12,14},{13,15},{18,16},{19,... | collective-permute-start | bytes 786440 | tf_op jit(solution)/shard_map/ppermute | solution.py:47
  172.6 6.0 %collective-permute-start.36 = (bf16[64,2048]{1,0:T(8,128)(2,1)S(1)}, bf16[64,2048]{1,0:T(8,128)(2,1)S(1)}, u32[]{:S(2)}, u32[]{:S(2)}) collective-permute-start(bf16[64,2048]{1,0:T(8,128)(2,1)S(1)} %add_convert_fusion.6), channel_id=1, source_target_pairs={{4,2},{5,3},{2,4},{3,5},{12,10},{13,11},{10,12},{11,13},{20,18},{2... | collective-permute-start | bytes 786440 | tf_op jit(solution)/shard_map/ppermute | solution.py:47
  173.3 10.5 %collective-permute-start.34 = (bf16[64,2048]{1,0:T(8,128)(2,1)S(1)}, bf16[64,2048]{1,0:T(8,128)(2,1)S(1)}, u32[]{:S(2)}, u32[]{:S(2)}) collective-permute-start(bf16[64,2048]{1,0:T(8,128)(2,1)S(1)} %add_convert_fusion.7), channel_id=1, source_target_pairs={{2,0},{3,1},{4,6},{5,7},{10,8},{11,9},{12,14},{13,15},{18,16},{19,... | collective-permute-start | bytes 786440 | tf_op jit(solution)/shard_map/ppermute | solution.py:47
  184.0 6.4 %collective-permute-start.37 = (bf16[32,2048]{1,0:T(8,128)(2,1)S(1)}, bf16[32,2048]{1,0:T(8,128)(2,1)S(1)}, u32[]{:S(2)}, u32[]{:S(2)}) collective-permute-start(bf16[32,2048]{1,0:T(8,128)(2,1)S(1)} %get-tuple-element.201), channel_id=1, source_target_pairs={{0,16},{8,24},{16,0},{24,8},{1,17},{9,25},{17,1},{25,9},{2,18},{10... | collective-permute-start | bytes 393224 | tf_op jit(solution)/shard_map/ppermute | solution.py:510
  184.3 6.1 %collective-permute-start.38 = (bf16[32,2048]{1,0:T(8,128)(2,1)S(1)}, bf16[32,2048]{1,0:T(8,128)(2,1)S(1)}, u32[]{:S(2)}, u32[]{:S(2)}) collective-permute-start(bf16[32,2048]{1,0:T(8,128)(2,1)S(1)} %get-tuple-element.200), channel_id=1, source_target_pairs={{0,24},{8,16},{16,8},{24,0},{1,25},{9,17},{17,9},{25,1},{2,26},{10... | collective-permute-start | bytes 393224 | tf_op jit(solution)/shard_map/ppermute | solution.py:510
  (16 other events, 154.9 us)
